TPU v7x, 32 devices: a whole 2x2x4 slice. The times are simulated.
32 devices in a mesh: ep: 8 (over z, core), tp: 4 (over y, x).
Axes of the slice: x: 2, y: 2, z: 4, core: 2. Of those that a mesh axis runs over, the one named last changes fastest.
Arguments:
- attn_in: bfloat16 [4096, 2048], P('ep'), may hold values from -6 to 6
- mix_gain: float32 [2048], replicated, may hold values from 0.1 to 1.9
- query_weight: bfloat16 [2048, 1024], P(None, 'tp'), may hold values from -0.125 to 0.125
- key_weight: bfloat16 [2048, 1024], P(None, 'tp'), may hold values from -0.125 to 0.125
- value_weight: bfloat16 [2048, 1024], P(None, 'tp'), may hold values from -0.125 to 0.125
- query_gain: float32 [64], replicated, may hold values from 0.7 to 6
- key_gain: float32 [64], replicated, may hold values from 0.7 to 6
- log_cache: float32 [4096, 16], P('ep', 'tp'), as said below
- head_gain: float32 [1024], P('tp'), may hold values from 0.1 to 1.9
- out_weight: bfloat16 [1024, 2048], P(None, 'tp'), may hold values from -0.1875 to 0.1875
- moe_in: bfloat16 [1024, 2048], P('ep'), may hold values from -6 to 6
- moe_gain: float32 [2048], replicated, may hold values from 0.1 to 1.9
- routes: int32 [1024, 2], P('ep'), may hold values from 0 to 7, all different within a row; in each aligned block of 128 rows (0 to 127, 128 to 255, ...) at most 48 rows name the same one
- route_weight: float32 [1024, 2], P('ep'), may hold values from 0.25 to 1
- expert_gate: bfloat16 [8, 2048, 1024], P('ep', None, 'tp'), may hold values from -0.125 to 0.125
- expert_up: bfloat16 [8, 2048, 1024], P('ep', None, 'tp'), may hold values from -0.125 to 0.125
- expert_down: bfloat16 [8, 1024, 2048], P('ep', 'tp'), may hold values from -0.1875 to 0.1875
Outputs:
- mixer_out: bfloat16 [4096, 2048], P('ep', 'tp')
- moe_out: bfloat16 [1024, 2048], P('ep', 'tp')
Inputs may be any that keep to these rules, and one draw needn't show every extreme that they name: `routes`: each row names 2 different experts; within the rows of one index of ep (aligned blocks of 128 rows) no expert is named by more than 48 rows. `log_cache`: never increasing along positions for each head.
All inputs are finite; a program needn't handle non-finite values.
Results may differ from a plain program's by a relative error of at most 0.015.
The roundings to bfloat16 on the way count: a program that leaves them out, or rounds other values in their place, can miss the bound.
Values may be sent and summed in bfloat16 or wider, within the bound.
A program may use at most 64 MiB of HBM per device.

v0:
```python
import math

import jax
import jax.numpy as jnp
from jax import lax
from jax.sharding import PartitionSpec as P

HD = 64


epsilon = 1e-06


def row_norm(inputs, gain_vec):
    floats = inputs.astype(jnp.float32)
    scaled = floats * lax.rsqrt(jnp.mean(floats * floats, axis=-1, keepdims=True) + epsilon)
    return scaled * gain_vec


def body(
    attn_in,
    mix_gain,
    query_weight,
    key_weight,
    value_weight,
    query_gain,
    key_gain,
    log_cache,
    head_gain,
    out_weight,
    moe_in,
    moe_gain,
    routes,
    route_weight,
    expert_gate,
    expert_up,
    expert_down,
):
    tok_rows = attn_in.shape[0]
    local_heads = query_weight.shape[1] // HD
    normed = row_norm(attn_in, mix_gain).astype(jnp.bfloat16)

    def project(weight):
        return jnp.dot(normed, weight, preferred_element_type=jnp.float32).reshape(
            tok_rows, local_heads, HD
        )

    queries = row_norm(project(query_weight), query_gain).astype(jnp.bfloat16)
    key_rows = (
        row_norm(project(key_weight), key_gain)
        .astype(jnp.bfloat16)
        .reshape(tok_rows, local_heads * HD)
    )
    value_rows = project(value_weight).astype(jnp.bfloat16).reshape(tok_rows, local_heads * HD)
    all_gates = lax.all_gather(log_cache, "ep", axis=0, tiled=True)
    query_pos = lax.axis_index("ep") * tok_rows + jnp.arange(tok_rows, dtype=jnp.int32)
    query_gates = jnp.transpose(log_cache)[:, :, None]
    score_scale = HD ** (-0.5)
    init_state = (
        jnp.full((local_heads, tok_rows), -1e30, jnp.float32),
        jnp.zeros((local_heads, tok_rows), jnp.float32),
        jnp.zeros((local_heads, tok_rows, HD), jnp.float32),
    )
    key_piece = lax.all_gather(key_rows, "ep", axis=0, tiled=True)
    value_piece = lax.all_gather(value_rows, "ep", axis=0, tiled=True)
    span_len = key_piece.shape[0]
    block_len = math.gcd(span_len, 512)

    def block_step(block_index, running):
        running_max, running_sum, weighted = running
        block_begin = block_index * block_len
        key_block = lax.dynamic_slice_in_dim(key_piece, block_begin, block_len, 0).reshape(
            block_len, local_heads, HD
        )
        value_block = lax.dynamic_slice_in_dim(value_piece, block_begin, block_len, 0).reshape(
            block_len, local_heads, HD
        )
        gate_block = lax.dynamic_slice_in_dim(all_gates, block_begin, block_len, 0)
        scores = (
            jnp.einsum("qhd,khd->hqk", queries, key_block, preferred_element_type=jnp.float32)
            * score_scale
        )
        scores = scores + query_gates - jnp.transpose(gate_block)[:, None, :]
        key_pos = block_begin + jnp.arange(block_len, dtype=jnp.int32)
        causal = (key_pos[None, :] <= query_pos[:, None])[None]
        new_max = jnp.maximum(running_max, jnp.max(jnp.where(causal, scores, -1e30), axis=2))
        expo_scores = jnp.where(causal, jnp.exp(scores - new_max[:, :, None]), 0.0)
        rescale = jnp.exp(running_max - new_max)
        running_sum = running_sum * rescale + jnp.sum(expo_scores, axis=2)
        weighted = weighted * rescale[:, :, None] + jnp.einsum(
            "hqk,khd->hqd",
            expo_scores.astype(jnp.bfloat16),
            value_block,
            preferred_element_type=jnp.float32,
        )
        return (new_max, running_sum, weighted)

    final_max, final_sum, weighted = lax.fori_loop(0, span_len // block_len, block_step, init_state)
    attended = jnp.transpose(weighted / final_sum[:, :, None], (1, 0, 2))
    head_out = (
        row_norm(attended, head_gain.reshape(local_heads, HD))
        .astype(jnp.bfloat16)
        .reshape(tok_rows, local_heads * HD)
    )
    mixer_out = jnp.dot(
        lax.all_gather(head_out, "tp", axis=1, tiled=True),
        out_weight,
        preferred_element_type=jnp.float32,
    ).astype(jnp.bfloat16)
    moe_rows = moe_in.shape[0]
    top_count = routes.shape[1]
    local_experts = expert_gate.shape[0]
    senders = lax.axis_size("ep")
    expert_count = local_experts * senders
    capacity = 3 * moe_rows * top_count // (2 * expert_count)
    model_width = moe_in.shape[1]
    moe_normed = row_norm(moe_in, moe_gain).astype(jnp.bfloat16)
    flat_routes = routes.reshape(-1)
    one_hot = (flat_routes[:, None] == jnp.arange(expert_count, dtype=jnp.int32)[None, :]).astype(
        jnp.int32
    )
    order_in = jnp.sum(jnp.cumsum(one_hot, axis=0) * one_hot, axis=1) - 1
    slot_index = flat_routes * capacity + order_in
    token_of = jnp.arange(flat_routes.shape[0], dtype=jnp.int32) // top_count
    source_row = jnp.zeros((expert_count * capacity,), jnp.int32).at[slot_index].set(token_of)
    filled = jnp.zeros((expert_count * capacity,), jnp.bool_).at[slot_index].set(True)
    send_buffer = jnp.where(
        filled[:, None], moe_normed[source_row], jnp.zeros((), jnp.bfloat16)
    ).reshape(expert_count, capacity, model_width)
    share_width = model_width // lax.axis_size("tp")
    share_part = lax.dynamic_slice_in_dim(
        send_buffer, lax.axis_index("tp") * share_width, share_width, 2
    )
    arrived = lax.all_to_all(share_part, "ep", split_axis=0, concat_axis=0, tiled=True)
    piece_now = lax.all_gather(arrived, "tp", axis=2, tiled=True)
    piece_cols = piece_now.shape[2]
    piece_rows = piece_now.reshape(senders, local_experts, capacity, piece_cols)
    gate_next = jnp.einsum(
        "sjcd,jdf->sjcf", piece_rows, expert_gate, preferred_element_type=jnp.float32
    )
    up_next = jnp.einsum(
        "sjcd,jdf->sjcf", piece_rows, expert_up, preferred_element_type=jnp.float32
    )
    hidden = (jax.nn.silu(gate_next) * up_next).astype(jnp.bfloat16)
    partial_value = jnp.einsum(
        "sjcf,jfd->sjcd", hidden, expert_down, preferred_element_type=jnp.float32
    )
    summed = lax.psum_scatter(
        partial_value.astype(jnp.bfloat16), "tp", scatter_dimension=3, tiled=True
    )
    out_cols = summed.shape[3]
    returned = lax.all_to_all(
        summed.reshape(expert_count, capacity, out_cols),
        "ep",
        split_axis=0,
        concat_axis=0,
        tiled=True,
    )
    picked = returned.reshape(expert_count * capacity, out_cols)[slot_index].astype(jnp.float32)
    weighted_rows = picked * route_weight.reshape(-1)[:, None]
    moe_out = jnp.sum(weighted_rows.reshape(moe_rows, top_count, out_cols), axis=1).astype(
        jnp.bfloat16
    )
    return (mixer_out, moe_out)


def solution(mesh):
    in_specs = (
        P("ep", None),
        P(),
        P(None, "tp"),
        P(None, "tp"),
        P(None, "tp"),
        P(),
        P(),
        P("ep", "tp"),
        P("tp"),
        P(None, "tp"),
        P("ep", None),
        P(),
        P("ep", None),
        P("ep", None),
        P("ep", None, "tp"),
        P("ep", None, "tp"),
        P("ep", "tp", None),
    )
    out_specs = (P("ep", "tp"), P("ep", "tp"))
    return jax.shard_map(body, mesh=mesh, in_specs=in_specs, out_specs=out_specs, check_vma=False)
```

profile of v0, /device:TPU:0, one launch (start us, length us, event | category | flops | bytes accessed | tf_op | source)
XLA Modules:
  0.0 263.2 jit_solution(7645723227461239029)
XLA Ops:
  18.4 18.8 %all_to_all.10 = bf16[8,48,512]{2,1,0:T(8,128)(2,1)} all-to-all(bf16[8,48,512]{2,1,0:T(8,128)(2,1)S(1)} %dynamic-slice_select_fusion), channel_id=1, replica_groups=mesh['ep'=8,'tp'=4] {'ep'}, dimensions={0} | all-to-all | bytes 786432 | tf_op jit(solution)/shard_map/all_to_all | solution.py:134
  46.3 14.0 %all_gather.16 = f32[4096,4]{0,1:T(4,128)S(1)} all-gather(f32[512,4]{0,1:T(4,128)S(1)} %copy-done.3), channel_id=1, replica_groups=mesh['ep'=8,'tp'=4] {'ep'}, dimensions={0}, use_global_device_ids=true | all-gather | bytes 73728 | tf_op jit(solution)/shard_map/all_gather | solution.py:55
  62.5 4.5 %all-gather.11.cloned.1.call-done = bf16[8,48,2048]{2,1,0:T(8,128)(2,1)} async-done(((bf16[8,48,512]{2,1,0:T(8,128)(2,1)}), bf16[8,48,2048]{2,1,0:T(8,128)(2,1)}) %all-gather.11.cloned.1.call-update) | async-done | bytes 1572880 | tf_op jit(solution)/shard_map/all_gather | solution.py:135
  69.3 4.8 %fusion.19 = bf16[8,1,48,2048]{3,2,0,1:T(8,128)(2,1)} fusion(bf16[1,256,2048]{2,1,0:T(8,128)(2,1)S(1)} %copy-done, bf16[8,48,2048]{2,1,0:T(8,128)(2,1)} %all-gather.11.cloned.1.call-done, bf16[1,2048,256]{2,1,0:T(8,128)(2,1)} %param.34, f32[8,1,48,256]{3,2,0,1:T(8,128)S(1)} %convolution_bitcast_fusion.1), kind=kOutput, calls=%fused_computation.35 | convolution fusion | flops 806682624 | bytes 5636096 | tf_op jit(solution)/shard_map/sjcf,jfd->sjcd/dot_general | solution.py:145
  74.4 23.4 %all-gather.5.cloned.1.call-done = bf16[4096,256]{0,1:T(8,128)(2,1)} async-done(((bf16[512,256]{0,1:T(8,128)(2,1)}), bf16[4096,256]{0,1:T(8,128)(2,1)}) %all-gather.5.cloned.1.call-update) | async-done | bytes 2097168 | tf_op jit(solution)/shard_map/all_gather | solution.py:64
  97.8 30.2 %all-gather.7.cloned.1.call-done = bf16[4096,256]{1,0:T(8,128)(2,1)} async-done(((bf16[512,256]{1,0:T(8,128)(2,1)}), bf16[4096,256]{1,0:T(8,128)(2,1)}) %all-gather.7.cloned.1.call-update) | async-done | bytes 2097168 | tf_op jit(solution)/shard_map/all_gather | solution.py:65
  128.0 95.6 %while.18 = (s32[]{:T(128)}, f32[4,512]{1,0:T(4,128)S(1)}, f32[4,512]{1,0:T(4,128)S(1)}, f32[4,512,64]{1,2,0:T(8,128)S(1)}, bf16[4096,256]{0,1:T(8,128)(2,1)}, /...) while((s32[]{:T(128)}, f32[4,512]{1,0:T(4,128)S(1)}, ...), condition=%wide.region_6.7_spmd.clone, body=%wide.region_3.6_spmd.clone.sunk | while | flops 286927872 | bytes 17244372 | solution.py:98
  129.2 3.1 %fusion.76 = (f32[4,512]{1,0:T(4,128)S(1)}, f32[4,512,512]{2,1,0:T(8,128)}) fusion(f32[4,512]{1,0:T(4,128)S(1)} %dynamic-slice_bitcast_fusion.2, f32[4,512]{1,0:T(4,128)S(1)} %bitcast.137, pred[512,512]{0,1:T(8,128)(4,1)S(1)} %broadcast_compare_fusion.2, bf16[512,4,64]{0,2,1:T(8,128)(2,1)S(1)} %bitcast.131, ...), kind=kOutput, calls=%fused_computation.7.clone.1 | convolution fusion | flops 139458560 | bytes 5005312 | tf_op jit(solution)/shard_map/while/body/eval_jaxpr/qhd,khd->hqk/dot_general | solution.py:80
  136.4 3.5 %fusion.79 = f32[4,512,64]{1,2,0:T(8,128)S(1)} fusion(bf16[512,4,64]{0,2,1:T(8,128)(2,1)S(1)} %bitcast.132, f32[4,512,512]{2,1,0:T(8,128)} %get-tuple-element.330, f32[4,512]{1,0:T(4,128)S(1)} %select_maximum_fusion.2, f32[4,512]{1,0:T(4,128)S(1)} %dynamic-slice_bitcast_fusion.2, f32[4,512]{1,0:T(4,128)S(1)} %bitcast.139, ...), kind=kOutput, calls=%fused_computation.15.clone.1 | convolution fusion | flops 140902400 | bytes 5799937 | tf_op jit(solution)/shard_map/while/body/eval_jaxpr/hqk,khd->hqd/dot_general | solution.py:90
  141.2 3.1 %fusion.76 = (f32[4,512]{1,0:T(4,128)S(1)}, f32[4,512,512]{2,1,0:T(8,128)}) fusion(f32[4,512]{1,0:T(4,128)S(1)} %dynamic-slice_bitcast_fusion.2, f32[4,512]{1,0:T(4,128)S(1)} %bitcast.137, pred[512,512]{0,1:T(8,128)(4,1)S(1)} %broadcast_compare_fusion.2, bf16[512,4,64]{0,2,1:T(8,128)(2,1)S(1)} %bitcast.131, ...), kind=kOutput, calls=%fused_computation.7.clone.1 | convolution fusion | flops 139458560 | bytes 5005312 | tf_op jit(solution)/shard_map/while/body/eval_jaxpr/qhd,khd->hqk/dot_general | solution.py:80
  148.4 3.5 %fusion.79 = f32[4,512,64]{1,2,0:T(8,128)S(1)} fusion(bf16[512,4,64]{0,2,1:T(8,128)(2,1)S(1)} %bitcast.132, f32[4,512,512]{2,1,0:T(8,128)} %get-tuple-element.330, f32[4,512]{1,0:T(4,128)S(1)} %select_maximum_fusion.2, f32[4,512]{1,0:T(4,128)S(1)} %dynamic-slice_bitcast_fusion.2, f32[4,512]{1,0:T(4,128)S(1)} %bitcast.139, ...), kind=kOutput, calls=%fused_computation.15.clone.1 | convolution fusion | flops 140902400 | bytes 5799937 | tf_op jit(solution)/shard_map/while/body/eval_jaxpr/hqk,khd->hqd/dot_general | solution.py:90
  153.2 3.1 %fusion.76 = (f32[4,512]{1,0:T(4,128)S(1)}, f32[4,512,512]{2,1,0:T(8,128)}) fusion(f32[4,512]{1,0:T(4,128)S(1)} %dynamic-slice_bitcast_fusion.2, f32[4,512]{1,0:T(4,128)S(1)} %bitcast.137, pred[512,512]{0,1:T(8,128)(4,1)S(1)} %broadcast_compare_fusion.2, bf16[512,4,64]{0,2,1:T(8,128)(2,1)S(1)} %bitcast.131, ...), kind=kOutput, calls=%fused_computation.7.clone.1 | convolution fusion | flops 139458560 | bytes 5005312 | tf_op jit(solution)/shard_map/while/body/eval_jaxpr/qhd,khd->hqk/dot_general | solution.py:80
  160.4 3.6 %fusion.79 = f32[4,512,64]{1,2,0:T(8,128)S(1)} fusion(bf16[512,4,64]{0,2,1:T(8,128)(2,1)S(1)} %bitcast.132, f32[4,512,512]{2,1,0:T(8,128)} %get-tuple-element.330, f32[4,512]{1,0:T(4,128)S(1)} %select_maximum_fusion.2, f32[4,512]{1,0:T(4,128)S(1)} %dynamic-slice_bitcast_fusion.2, f32[4,512]{1,0:T(4,128)S(1)} %bitcast.139, ...), kind=kOutput, calls=%fused_computation.15.clone.1 | convolution fusion | flops 140902400 | bytes 5799937 | tf_op jit(solution)/shard_map/while/body/eval_jaxpr/hqk,khd->hqd/dot_general | solution.py:90
  165.2 3.1 %fusion.76 = (f32[4,512]{1,0:T(4,128)S(1)}, f32[4,512,512]{2,1,0:T(8,128)}) fusion(f32[4,512]{1,0:T(4,128)S(1)} %dynamic-slice_bitcast_fusion.2, f32[4,512]{1,0:T(4,128)S(1)} %bitcast.137, pred[512,512]{0,1:T(8,128)(4,1)S(1)} %broadcast_compare_fusion.2, bf16[512,4,64]{0,2,1:T(8,128)(2,1)S(1)} %bitcast.131, ...), kind=kOutput, calls=%fused_computation.7.clone.1 | convolution fusion | flops 139458560 | bytes 5005312 | tf_op jit(solution)/shard_map/while/body/eval_jaxpr/qhd,khd->hqk/dot_general | solution.py:80
  172.3 3.5 %fusion.79 = f32[4,512,64]{1,2,0:T(8,128)S(1)} fusion(bf16[512,4,64]{0,2,1:T(8,128)(2,1)S(1)} %bitcast.132, f32[4,512,512]{2,1,0:T(8,128)} %get-tuple-element.330, f32[4,512]{1,0:T(4,128)S(1)} %select_maximum_fusion.2, f32[4,512]{1,0:T(4,128)S(1)} %dynamic-slice_bitcast_fusion.2, f32[4,512]{1,0:T(4,128)S(1)} %bitcast.139, ...), kind=kOutput, calls=%fused_computation.15.clone.1 | convolution fusion | flops 140902400 | bytes 5799937 | tf_op jit(solution)/shard_map/while/body/eval_jaxpr/hqk,khd->hqd/dot_general | solution.py:90
  177.1 3.1 %fusion.76 = (f32[4,512]{1,0:T(4,128)S(1)}, f32[4,512,512]{2,1,0:T(8,128)}) fusion(f32[4,512]{1,0:T(4,128)S(1)} %dynamic-slice_bitcast_fusion.2, f32[4,512]{1,0:T(4,128)S(1)} %bitcast.137, pred[512,512]{0,1:T(8,128)(4,1)S(1)} %broadcast_compare_fusion.2, bf16[512,4,64]{0,2,1:T(8,128)(2,1)S(1)} %bitcast.131, ...), kind=kOutput, calls=%fused_computation.7.clone.1 | convolution fusion | flops 139458560 | bytes 5005312 | tf_op jit(solution)/shard_map/while/body/eval_jaxpr/qhd,khd->hqk/dot_general | solution.py:80
  184.3 3.5 %fusion.79 = f32[4,512,64]{1,2,0:T(8,128)S(1)} fusion(bf16[512,4,64]{0,2,1:T(8,128)(2,1)S(1)} %bitcast.132, f32[4,512,512]{2,1,0:T(8,128)} %get-tuple-element.330, f32[4,512]{1,0:T(4,128)S(1)} %select_maximum_fusion.2, f32[4,512]{1,0:T(4,128)S(1)} %dynamic-slice_bitcast_fusion.2, f32[4,512]{1,0:T(4,128)S(1)} %bitcast.139, ...), kind=kOutput, calls=%fused_computation.15.clone.1 | convolution fusion | flops 140902400 | bytes 5799937 | tf_op jit(solution)/shard_map/while/body/eval_jaxpr/hqk,khd->hqd/dot_general | solution.py:90
  189.0 3.1 %fusion.76 = (f32[4,512]{1,0:T(4,128)S(1)}, f32[4,512,512]{2,1,0:T(8,128)}) fusion(f32[4,512]{1,0:T(4,128)S(1)} %dynamic-slice_bitcast_fusion.2, f32[4,512]{1,0:T(4,128)S(1)} %bitcast.137, pred[512,512]{0,1:T(8,128)(4,1)S(1)} %broadcast_compare_fusion.2, bf16[512,4,64]{0,2,1:T(8,128)(2,1)S(1)} %bitcast.131, ...), kind=kOutput, calls=%fused_computation.7.clone.1 | convolution fusion | flops 139458560 | bytes 5005312 | tf_op jit(solution)/shard_map/while/body/eval_jaxpr/qhd,khd->hqk/dot_general | solution.py:80
  196.2 3.5 %fusion.79 = f32[4,512,64]{1,2,0:T(8,128)S(1)} fusion(bf16[512,4,64]{0,2,1:T(8,128)(2,1)S(1)} %bitcast.132, f32[4,512,512]{2,1,0:T(8,128)} %get-tuple-element.330, f32[4,512]{1,0:T(4,128)S(1)} %select_maximum_fusion.2, f32[4,512]{1,0:T(4,128)S(1)} %dynamic-slice_bitcast_fusion.2, f32[4,512]{1,0:T(4,128)S(1)} %bitcast.139, ...), kind=kOutput, calls=%fused_computation.15.clone.1 | convolution fusion | flops 140902400 | bytes 5799937 | tf_op jit(solution)/shard_map/while/body/eval_jaxpr/hqk,khd->hqd/dot_general | solution.py:90
  201.0 3.1 %fusion.76 = (f32[4,512]{1,0:T(4,128)S(1)}, f32[4,512,512]{2,1,0:T(8,128)}) fusion(f32[4,512]{1,0:T(4,128)S(1)} %dynamic-slice_bitcast_fusion.2, f32[4,512]{1,0:T(4,128)S(1)} %bitcast.137, pred[512,512]{0,1:T(8,128)(4,1)S(1)} %broadcast_compare_fusion.2, bf16[512,4,64]{0,2,1:T(8,128)(2,1)S(1)} %bitcast.131, ...), kind=kOutput, calls=%fused_computation.7.clone.1 | convolution fusion | flops 139458560 | bytes 5005312 | tf_op jit(solution)/shard_map/while/body/eval_jaxpr/qhd,khd->hqk/dot_general | solution.py:80
  208.1 3.5 %fusion.79 = f32[4,512,64]{1,2,0:T(8,128)S(1)} fusion(bf16[512,4,64]{0,2,1:T(8,128)(2,1)S(1)} %bitcast.132, f32[4,512,512]{2,1,0:T(8,128)} %get-tuple-element.330, f32[4,512]{1,0:T(4,128)S(1)} %select_maximum_fusion.2, f32[4,512]{1,0:T(4,128)S(1)} %dynamic-slice_bitcast_fusion.2, f32[4,512]{1,0:T(4,128)S(1)} %bitcast.139, ...), kind=kOutput, calls=%fused_computation.15.clone.1 | convolution fusion | flops 140902400 | bytes 5799937 | tf_op jit(solution)/shard_map/while/body/eval_jaxpr/hqk,khd->hqd/dot_general | solution.py:90
  220.1 3.5 %fusion.79 = f32[4,512,64]{1,2,0:T(8,128)S(1)} fusion(bf16[512,4,64]{0,2,1:T(8,128)(2,1)S(1)} %bitcast.132, f32[4,512,512]{2,1,0:T(8,128)} %get-tuple-element.330, f32[4,512]{1,0:T(4,128)S(1)} %select_maximum_fusion.2, f32[4,512]{1,0:T(4,128)S(1)} %dynamic-slice_bitcast_fusion.2, f32[4,512]{1,0:T(4,128)S(1)} %bitcast.139, ...), kind=kOutput, calls=%fused_computation.15.clone.1 | convolution fusion | flops 140902400 | bytes 5799937 | tf_op jit(solution)/shard_map/while/body/eval_jaxpr/hqk,khd->hqd/dot_general | solution.py:90
  224.6 3.5 %all-to-all-start.1 = ((bf16[8,48,512]{2,1,0:T(8,128)(2,1)}), bf16[8,48,512]{2,1,0:T(8,128)(2,1)S(1)}, u32[]{:S(2)}, u32[]{:S(2)}) async-start(bf16[8,48,512]{2,1,0:T(8,128)(2,1)} %bitcast.135), calls=%async_computation.2 | async-start | bytes 786432 | tf_op jit(solution)/shard_map/all_to_all | solution.py:152
  228.2 22.6 %all-gather.9.cloned.1.call-done = bf16[512,1024]{0,1:T(8,128)(2,1)} async-done(((bf16[512,256]{0,1:T(8,128)(2,1)}), bf16[512,1024]{0,1:T(8,128)(2,1)}) %all-gather.9.cloned.1.call-update) | async-done | bytes 1048592 | tf_op jit(solution)/shard_map/all_gather | solution.py:106
  (162 shorter events, 77.2 us)
Async XLA Ops:
  7.2 62.1 %copy-start = (bf16[1,256,2048]{2,1,0:T(8,128)(2,1)S(1)}, bf16[1,256,2048]{2,1,0:T(8,128)(2,1)}, u32[]{:S(2)}) copy-start(bf16[1,256,2048]{2,1,0:T(8,128)(2,1)} %param.35) | copy-start | bytes 3145732
  7.2 59.9 %all-gather.11.cloned.1.call-start = ((), (), s32[]{:S(2)}) async-start(), calls=%async_computation.6 | async-start | bytes 1966080 | tf_op jit(solution)/shard_map/all_gather | solution.py:135
  15.8 21.5 %copy-start.6 = (f32[64]{0:T(128)S(1)}, f32[64]{0:T(128)}, u32[]{:S(2)}) copy-start(f32[64]{0:T(128)} %param.25) | copy-start | bytes 772
  15.8 23.8 %copy-start.8 = (f32[2048]{0:T(1024)S(1)}, f32[2048]{0:T(1024)}, u32[]{:S(2)}) copy-start(f32[2048]{0:T(1024)} %param.20) | copy-start | bytes 24580
  37.2 60.6 %all-gather.5.cloned.1.call-start = ((), (), s32[]{:S(2)}) async-start(), calls=%async_computation.3 | async-start | bytes 2359296 | tf_op jit(solution)/shard_map/all_gather | solution.py:64
  37.4 6.0 %copy-start.1 = (bf16[512,2048]{1,0:T(8,128)(2,1)S(1)}, bf16[512,2048]{1,0:T(8,128)(2,1)}, u32[]{:S(2)}) copy-start(bf16[512,2048]{1,0:T(8,128)(2,1)} %param.19) | copy-start | bytes 6291460
  42.4 3.8 %copy-start.5 = (f32[256]{0:T(256)S(1)}, f32[256]{0:T(256)}, u32[]{:S(2)}) copy-start(f32[256]{0:T(256)} %param.27) | copy-start | bytes 3076
  42.4 3.8 %copy-start.3 = (f32[512,4]{0,1:T(4,128)S(1)}, f32[512,4]{0,1:T(4,128)}, u32[]{:S(2)}) copy-start(f32[512,4]{0,1:T(4,128)} %param.26) | copy-start | bytes 24580
  43.3 84.7 %all-gather.7.cloned.1.call-start = ((), (), s32[]{:S(2)}) async-start(), calls=%async_computation.4 | async-start | bytes 2359296 | tf_op jit(solution)/shard_map/all_gather | solution.py:65
  46.1 16.4 %copy-start.7 = (f32[64]{0:T(128)S(1)}, f32[64]{0:T(128)}, u32[]{:S(2)}) copy-start(f32[64]{0:T(128)} %param.24) | copy-start | bytes 772
  46.1 178.5 %reduce-scatter.2.cloned.1.call-start = ((), (), s32[]{:S(2)}) async-start(), calls=%async_computation.7 | async-start | bytes 1966080 | tf_op jit(solution)/shard_map/reduce_scatter | solution.py:148
  69.3 58.7 %copy-start.2 = (f32[4,512,64]{1,2,0:T(8,128)S(1)}, f32[4,512,64]{1,2,0:T(8,128)}, u32[]{:S(2)}) copy-start(f32[4,512,64]{1,2,0:T(8,128)} %custom-call.2) | copy-start | bytes 1572868
  74.1 176.6 %all-gather.9.cloned.1.call-start = ((), (), s32[]{:S(2)}) async-start(), calls=%async_computation.5 | async-start | bytes 1310720 | tf_op jit(solution)/shard_map/all_gather | solution.py:106
  128.0 100.0 %copy-start.4 = (f32[128,2]{0,1:T(2,128)S(1)}, f32[128,2]{0,1:T(2,128)}, u32[]{:S(2)}) copy-start(f32[128,2]{0,1:T(2,128)} %param.32) | copy-start | bytes 3076
  224.6 29.3 %all-to-all-start.1 = ((bf16[8,48,512]{2,1,0:T(8,128)(2,1)}), bf16[8,48,512]{2,1,0:T(8,128)(2,1)S(1)}, u32[]{:S(2)}, u32[]{:S(2)}) async-start(bf16[8,48,512]{2,1,0:T(8,128)(2,1)} %bitcast.135), calls=%async_computation.2 | async-start | bytes 786432 | tf_op jit(solution)/shard_map/all_to_all | solution.py:152
Sparse Core Ops, SparseCore 0:
  37.3 29.6 all-gather.10
  68.6 29.1 all-gather.4
  99.4 28.5 all-gather.6
  130.8 30.5 reduce-scatter.1
  224.6 26.0 all-gather.8
where the time goes:
time: 265 us; the launch traced here: 263 us
  waiting for transfers between devices  80.8 us (30%)
  matrix products  70.6 us (27%)
  other arithmetic  34.9 us (13%)
  blocking collectives  32.8 us (12%)
  local copies, waits for them, and re-layouts  25.7 us (10%)
  between operations  14.1 us (5%)
  starting transfers between devices  3.85 us (1%)
    all_gather x1, waiting for transfers between devices, body(): value_piece = lax.all_gather(value_rows, 'ep', axis=0, tiled=True)  30.2 us
    dot_general x8, matrix products, block_step(): jnp.einsum('hqk,khd->hqd', expo_scores.astype(jnp.bfloat16), value_block,...  28.1 us
    dot_general x8, matrix products, block_step(): jnp.einsum('qhd,khd->hqk', queries, key_block, preferred_element_type=jnp...  24.7 us
    all_gather x1, waiting for transfers between devices, body(): key_piece = lax.all_gather(key_rows, 'ep', axis=0, tiled=True)  23.4 us
    reduce_sum x8, other arithmetic, block_step(): running_sum = running_sum * rescale + jnp.sum(expo_scores, axis=2)  23.4 us
    all_gather x1, waiting for transfers between devices, body(): lax.all_gather(head_out, 'tp', axis=1, tiled=True)  22.6 us
    all_to_all x1, blocking collectives, body(): lax.all_to_all(share_part, 'ep', split_axis=0, concat_axis=0, tiled=True)  18.8 us
    all_gather x1, blocking collectives, body(): all_gates = lax.all_gather(log_cache, 'ep', axis=0, tiled=True)  14 us
  transfers between devices with their start and end apart: 6, of which 4 were waited for; matrix products, arithmetic and copies ran while one was open for 45% of the time, Pallas kernels for 0%

commit v1 on v0

v1 whole, which is shorter than its diff:
```python
import functools

import jax
import jax.numpy as jnp
from jax import lax
from jax.experimental import pallas as pl
from jax.experimental.pallas import tpu as pltpu
from jax.sharding import PartitionSpec as P

HD = 64
LANES = 128
epsilon = 1e-06
BF = jnp.bfloat16
F32 = jnp.float32


def row_norm(inputs, gain_vec):
    floats = inputs.astype(F32)
    scaled = floats * lax.rsqrt(jnp.mean(floats * floats, axis=-1, keepdims=True) + epsilon)
    return scaled * gain_vec


def split3(x):
    hi = lax.reduce_precision(x, 8, 7)
    rest = x - hi
    mid = lax.reduce_precision(rest, 8, 7)
    return hi.astype(BF), mid.astype(BF), (rest - mid).astype(BF)


def attend_kernel(heads, q_ref, k_ref, v_ref, aug_ref, gain_ref, o_ref, qz, m_s, l_s, acc):
    me = lax.axis_index("ep")
    tok = q_ref.shape[1]
    row = lax.broadcasted_iota(jnp.int32, (LANES, tok), 0)
    zeros = jnp.zeros((HD, tok), BF)
    for h in range(heads):
        q_h = q_ref[h * HD:(h + 1) * HD, :]
        parts = [q_h, zeros] if h % 2 == 0 else [zeros, q_h]
        pick = jnp.where((row >= 3 * h) & (row < 3 * h + 3), -1.0, 0.0).astype(BF)
        qz[h] = jnp.concatenate(parts + [pick], axis=0)

    def step(block, first, masked):
        aug = aug_ref[block]
        for h in range(heads):
            p = h // 2
            keys = jnp.concatenate([k_ref[block, :, p * LANES:(p + 1) * LANES], aug], axis=1)
            s = jnp.dot(keys, qz[h], preferred_element_type=F32)
            if masked:
                kpos = lax.broadcasted_iota(jnp.int32, s.shape, 0)
                qpos = lax.broadcasted_iota(jnp.int32, s.shape, 1)
                s = jnp.where(kpos <= qpos, s, -1e30)
            top = jnp.max(s, axis=0, keepdims=True)
            if first:
                new = top
            else:
                new = jnp.maximum(m_s[h], top)
            e = jnp.exp(s - new)
            total = jnp.sum(e, axis=0, keepdims=True)
            o = jnp.dot(v_ref[block, h * HD:(h + 1) * HD, :], e.astype(BF), preferred_element_type=F32)
            if first:
                l_s[h] = total
                acc[h] = o
            else:
                fix = jnp.exp(m_s[h] - new)
                l_s[h] = l_s[h] * fix + total
                acc[h] = acc[h] * fix + o
            m_s[h] = new

    step(me, True, True)

    @pl.loop(0, me)
    def _(i):
        step(i, False, False)

    for h in range(heads):
        a = acc[h] / l_s[h]
        a = a * lax.rsqrt(jnp.mean(a * a, axis=0, keepdims=True) + epsilon)
        o_ref[h * HD:(h + 1) * HD, :] = (a * gain_ref[h * HD:(h + 1) * HD, :]).astype(BF)


def attend(q_t, k_all, v_all, aug, gain):
    feats, tok = q_t.shape
    heads = feats // HD
    vm = pl.BlockSpec(memory_space=pltpu.VMEM)
    blocks = k_all.shape[0]
    scores = heads * blocks * tok * tok
    return pl.pallas_call(
        functools.partial(attend_kernel, heads),
        out_shape=jax.ShapeDtypeStruct((feats, tok), BF),
        in_specs=[vm] * 5,
        out_specs=vm,
        scratch_shapes=[
            pltpu.VMEM((heads, 2 * LANES, tok), BF),
            pltpu.VMEM((heads, 1, tok), F32),
            pltpu.VMEM((heads, 1, tok), F32),
            pltpu.VMEM((heads, HD, tok), F32),
        ],
        compiler_params=pltpu.CompilerParams(vmem_limit_bytes=56 * 1024 * 1024),
        cost_estimate=pl.CostEstimate(flops=scores * 512, bytes_accessed=2**23, transcendentals=scores),
    )(q_t, k_all, v_all, aug, gain)


def body(
    attn_in,
    mix_gain,
    query_weight,
    key_weight,
    value_weight,
    query_gain,
    key_gain,
    log_cache,
    head_gain,
    out_weight,
    moe_in,
    moe_gain,
    routes,
    route_weight,
    expert_gate,
    expert_up,
    expert_down,
):
    tok_rows = attn_in.shape[0]
    feats = query_weight.shape[1]
    local_heads = feats // HD
    normed = row_norm(attn_in, mix_gain).astype(BF)

    def project(weight):
        return lax.dot_general(weight, normed, (((0,), (1,)), ((), ())), preferred_element_type=F32)

    def head_norm(x, gain):
        x = x.reshape(local_heads, HD, tok_rows)
        x = x * lax.rsqrt(jnp.mean(x * x, axis=1, keepdims=True) + epsilon)
        return (x * gain[None, :, None]).astype(BF).reshape(feats, tok_rows)

    k_rows = jnp.transpose(head_norm(project(key_weight), key_gain))
    if feats % LANES:
        k_rows = jnp.pad(k_rows, ((0, 0), (0, LANES - feats % LANES)))
    v_t = project(value_weight).astype(BF)
    k_all = lax.all_gather(k_rows, "ep")
    v_all = lax.all_gather(v_t, "ep")
    q_t = head_norm(project(query_weight), query_gain) * jnp.asarray(HD ** -0.5, BF)
    gates = lax.all_gather(log_cache, "ep")
    hi, mid, low = split3(gates)
    aug = jnp.stack([hi, mid, low], axis=-1).reshape(gates.shape[0], tok_rows, 3 * local_heads)
    aug = jnp.pad(aug, ((0, 0), (0, 0), (0, LANES - 3 * local_heads)))
    head_t = attend(q_t, k_all, v_all, aug, head_gain[:, None])
    mixer_out = lax.dot_general(
        lax.all_gather(head_t, "tp", axis=0, tiled=True),
        out_weight,
        (((0,), (0,)), ((), ())),
        preferred_element_type=F32,
    ).astype(BF)

    moe_rows = moe_in.shape[0]
    top_count = routes.shape[1]
    local_experts = expert_gate.shape[0]
    senders = lax.axis_size("ep")
    expert_count = local_experts * senders
    capacity = 3 * moe_rows * top_count // (2 * expert_count)
    model_width = moe_in.shape[1]
    moe_normed = row_norm(moe_in, moe_gain).astype(BF)
    flat_routes = routes.reshape(-1)
    one_hot = (flat_routes[:, None] == jnp.arange(expert_count, dtype=jnp.int32)[None, :]).astype(
        jnp.int32
    )
    order_in = jnp.sum(jnp.cumsum(one_hot, axis=0) * one_hot, axis=1) - 1
    slot_index = flat_routes * capacity + order_in
    slots = jnp.arange(expert_count * capacity, dtype=jnp.int32)
    hit = (slots[:, None, None] == slot_index.reshape(1, moe_rows, top_count)).any(axis=2)
    share_width = model_width // lax.axis_size("tp")
    my_share = lax.dynamic_slice_in_dim(moe_normed, lax.axis_index("tp") * share_width, share_width, 1)
    share_part = (
        jnp.dot(hit.astype(BF), my_share, preferred_element_type=F32)
        .astype(BF)
        .reshape(expert_count, capacity, share_width)
    )
    arrived = lax.all_to_all(share_part, "ep", split_axis=0, concat_axis=0, tiled=True)
    piece_now = lax.all_gather(arrived, "tp", axis=2, tiled=True)
    piece_cols = piece_now.shape[2]
    piece_rows = piece_now.reshape(senders, local_experts, capacity, piece_cols)
    gate_next = jnp.einsum("sjcd,jdf->sjcf", piece_rows, expert_gate, preferred_element_type=F32)
    up_next = jnp.einsum("sjcd,jdf->sjcf", piece_rows, expert_up, preferred_element_type=F32)
    hidden = (jax.nn.silu(gate_next) * up_next).astype(BF)
    partial_value = jnp.einsum("sjcf,jfd->sjcd", hidden, expert_down, preferred_element_type=F32)
    summed = lax.psum_scatter(partial_value.astype(BF), "tp", scatter_dimension=3, tiled=True)
    out_cols = summed.shape[3]
    returned = lax.all_to_all(
        summed.reshape(expert_count, capacity, out_cols),
        "ep",
        split_axis=0,
        concat_axis=0,
        tiled=True,
    )
    flat = returned.reshape(expert_count * capacity, out_cols)
    pick = (slot_index[:, None] == slots[None, :]).astype(BF)
    picked = jnp.dot(pick, flat, preferred_element_type=F32)
    weighted_rows = picked * route_weight.reshape(-1)[:, None]
    moe_out = jnp.sum(weighted_rows.reshape(moe_rows, top_count, out_cols), axis=1).astype(BF)
    return (mixer_out, moe_out)


def solution(mesh):
    in_specs = (
        P("ep", None),
        P(),
        P(None, "tp"),
        P(None, "tp"),
        P(None, "tp"),
        P(),
        P(),
        P("ep", "tp"),
        P("tp"),
        P(None, "tp"),
        P("ep", None),
        P(),
        P("ep", None),
        P("ep", None),
        P("ep", None, "tp"),
        P("ep", None, "tp"),
        P("ep", "tp", None),
    )
    out_specs = (P("ep", "tp"), P("ep", "tp"))
    return jax.shard_map(body, mesh=mesh, in_specs=in_specs, out_specs=out_specs, check_vma=False)
```

time: 265 us -> 199 us (0.75)
  matrix products: 70.6 us -> 16.8 us
  other arithmetic: 34.9 us -> 8.29 us
  waiting for transfers between devices: 80.8 us -> 101 us
  local copies, waits for them, and re-layouts: 25.7 us -> 14.6 us
  Pallas kernels: 0 us -> 5.39 us
    dot_general x20 -> x6, matrix products: 63.5 us -> 10.2 us  [the longest x3 5.83 us: project(): lax.dot_general(weight, normed, (((0,), (1,)), ((), ())), preferred_eleme...]
    reduce_scatter x1, waiting for transfers between devices: 0.02 us -> 23.7 us  [body(): lax.psum_scatter(partial_value.astype(BF), 'tp', scatter_dimension=3, til...]
    reduce_sum x8 -> x0, other arithmetic: 23.4 us -> none  [block_step(): running_sum = running_sum * rescale + jnp.sum(expo_scores, axis=2)]
    all_gather x3, waiting for transfers between devices: 76.2 us -> 54.5 us  [the longest x1 27.4 us: body(): v_all = lax.all_gather(v_t, 'ep')]
    all_gather x1, waiting for transfers between devices: 4.48 us -> 22.8 us  [body(): piece_now = lax.all_gather(arrived, 'tp', axis=2, tiled=True)]
    dynamic_slice x24 -> x1, local copies, waits for them, and re-layouts: 16.7 us -> 0.92 us  [body(): lax.dynamic_slice_in_dim(moe_normed, lax.axis_index('tp') * share_width,...]
    all_gather x0 -> x2, local copies, waits for them, and re-layouts: none -> 7.99 us  [the longest x1 4.07 us: body(): k_all = lax.all_gather(k_rows, 'ep')]
    pallas_call x0 -> x1, Pallas kernels: none -> 5.39 us  [attend(): pl.pallas_call(functools.partial(attend_kernel, heads), out_shape=jax.Sha...]
  transfers between devices with their start and end apart: 6 -> 6, of which waited for: 4 -> 5; matrix products, arithmetic and copies ran while one was open for 45% -> 15% of each run, Pallas kernels for 0% -> 3%
where the time goes in v1:
time: 199 us; the launch traced here: 198 us
  waiting for transfers between devices  101 us (51%)
  blocking collectives  33.1 us (17%)
  matrix products  16.8 us (8%)
  local copies, waits for them, and re-layouts  14.6 us (7%)
  between operations  14 us (7%)
  other arithmetic  8.29 us (4%)
  Pallas kernels  5.39 us (3%)
  starting transfers between devices  4.79 us (2%)
    all_gather x1, waiting for transfers between devices, body(): v_all = lax.all_gather(v_t, 'ep')  27.4 us
    reduce_scatter x1, waiting for transfers between devices, body(): lax.psum_scatter(partial_value.astype(BF), 'tp', scatter_dimension=3, til...  23.7 us
    all_gather x1, waiting for transfers between devices, body(): lax.all_gather(head_t, 'tp', axis=0, tiled=True)  23.4 us
    all_gather x1, waiting for transfers between devices, body(): piece_now = lax.all_gather(arrived, 'tp', axis=2, tiled=True)  22.8 us
    all_to_all x1, blocking collectives, body(): lax.all_to_all(share_part, 'ep', split_axis=0, concat_axis=0, tiled=True)  18.8 us
    all_gather x1, blocking collectives, body(): gates = lax.all_gather(log_cache, 'ep')  14.3 us
    dot_general x3, matrix products, project(): lax.dot_general(weight, normed, (((0,), (1,)), ((), ())), preferred_eleme...  5.83 us
    pallas_call x1, Pallas kernels, attend(): pl.pallas_call(functools.partial(attend_kernel, heads), out_shape=jax.Sha...  5.39 us
  transfers between devices with their start and end apart: 6, of which 5 were waited for; matrix products, arithmetic and copies ran while one was open for 15% of the time, Pallas kernels for 3%

profile of v1, /device:TPU:0, one launch (start us, length us, event | category | flops | bytes accessed | tf_op | source)
XLA Modules:
  0.0 198.1 jit_solution(6098780866631577232)
XLA Ops:
  7.2 0.9 copy.52
  8.5 2.1 %convert_element_type.79 = f32[128,2048]{1,0:T(8,128)} convert(bf16[128,2048]{1,0:T(8,128)(2,1)} %param.27) | non-fusion elementwise | flops 262144 | bytes 1572864 | tf_op jit(solution)/shard_map/convert_element_type | solution.py:18
  12.0 0.9 dynamic-slice
  13.0 1.3 convolution_convert_fusion.2
  14.2 18.8 %all_to_all.10 = bf16[8,48,512]{2,1,0:T(8,128)(2,1)} all-to-all(bf16[8,48,512]{2,1,0:T(8,128)(2,1)S(1)} %bitcast.118), channel_id=1, replica_groups=mesh['ep'=8,'tp'=4] {'ep'}, dimensions={0} | all-to-all | bytes 786432 | tf_op jit(solution)/shard_map/all_to_all | solution.py:176
  33.2 2.2 %fusion = f32[512]{0:T(512)S(1)} fusion(bf16[512,2048]{1,0:T(8,128)(2,1)} %param.17), kind=kLoop, calls=%fused_computation.2 | loop fusion | flops 3145216 | bytes 2099200 | tf_op jit(solution)/shard_map/reduce_sum | solution.py:19
  35.4 0.9 bitcast_reduce_fusion
  37.3 2.7 %fusion.6 = bf16[256,512]{0,1:T(8,128)(2,1)} fusion(bf16[2048,256]{1,0:T(8,128)(2,1)} %param.21, bf16[512,2048]{1,0:T(8,128)(2,1)S(1)} %copy-done.2, f32[2048]{0:T(1024)S(1)} %copy-done.13, f32[512]{0:T(512)S(1)} %add_rsqrt_fusion.2), kind=kOutput, calls=%fused_computation.17 | convolution fusion | flops 541196288 | bytes 3418112 | tf_op jit(solution)/shard_map/dot_general | solution.py:127
  40.0 22.8 %all-gather.10.cloned.1.call-done = bf16[8,48,2048]{2,1,0:T(8,128)(2,1)} async-done(((bf16[8,48,512]{2,1,0:T(8,128)(2,1)}), bf16[8,48,2048]{2,1,0:T(8,128)(2,1)}) %all-gather.10.cloned.1.call-update) | async-done | bytes 1572880 | tf_op jit(solution)/shard_map/all_gather | solution.py:177
  62.8 2.4 %convolution_bitcast_fusion.3 = f32[8,1,48,256]{3,2,0,1:T(8,128)S(1)} fusion(bf16[8,48,2048]{2,1,0:T(8,128)(2,1)} %all-gather.10.cloned.1.call-done, bf16[1,2048,256]{2,1,0:T(8,128)(2,1)} %param.31), kind=kOutput, calls=%fused_computation.14 | convolution fusion | flops 402653184 | bytes 3014656 | tf_op jit(solution)/shard_map/sjcd,jdf->sjcf/dot_general | solution.py:180
  65.3 4.2 %fusion.3 = bf16[8,1,48,2048]{3,2,0,1:T(8,128)(2,1)} fusion(bf16[1,256,2048]{2,1,0:T(8,128)(2,1)S(1)} %copy-done, bf16[8,48,2048]{2,1,0:T(8,128)(2,1)S(1)} %copy-done.4, bf16[1,2048,256]{2,1,0:T(8,128)(2,1)} %param.32, f32[8,1,48,256]{3,2,0,1:T(8,128)S(1)} %convolution_bitcast_fusion.3), kind=kOutput, calls=%fused_computation.6 | convolution fusion | flops 806682624 | bytes 5636096 | tf_op jit(solution)/shard_map/sjcf,jfd->sjcd/dot_general | solution.py:183
  69.7 14.3 %all-gather.2 = f32[4096,4]{0,1:T(4,128)S(1)} all-gather(f32[512,4]{0,1:T(4,128)S(1)} %copy-done.5), channel_id=4, replica_groups=mesh['ep'=8,'tp'=4] {'ep'}, dimensions={0}, use_global_device_ids=true | all-gather | bytes 73728 | tf_op jit(solution)/shard_map/all_gather | solution.py:141
  85.4 1.3 pad.4.aug_ref
  87.3 2.2 %bitcast_reduce_fusion.1 = (f32[4,512]{1,0:T(4,128)S(1)}, f32[256,512]{1,0:T(8,128)S(1)}) fusion(bf16[2048,256]{1,0:T(8,128)(2,1)} %param.19, bf16[512,2048]{1,0:T(8,128)(2,1)S(1)} %copy-done.3, f32[2048]{0:T(1024)S(1)} %copy-done.13, f32[512]{0:T(512)S(1)} %add_rsqrt_fusion.2), kind=kOutput, calls=%fused_computation.30 | convolution fusion | flops 541325312 | bytes 3688448 | tf_op jit(solution)/shard_map/dot_general | solution.py:127
  90.4 3.8 %all-gather.12.cloned.1.call-done = bf16[4096,256]{0,1:T(8,128)(2,1)} async-done(((bf16[512,256]{0,1:T(8,128)(2,1)}), bf16[4096,256]{0,1:T(8,128)(2,1)}) %all-gather.12.cloned.1.call-update) | async-done | bytes 2097168 | tf_op jit(solution)/shard_map/all_gather | solution.py:138
  94.1 4.1 %copy.47 = bf16[4096,256]{1,0:T(8,128)(2,1)} copy(bf16[4096,256]{0,1:T(8,128)(2,1)} %all-gather.12.cloned.1.call-done) | data formatting | bytes 4194304 | tf_op jit(solution)/shard_map/all_gather | solution.py:138
  98.2 27.4 %all-gather.14.cloned.1.call-done = bf16[2048,512]{0,1:T(8,128)(2,1)} async-done(((bf16[256,512]{0,1:T(8,128)(2,1)}), bf16[2048,512]{0,1:T(8,128)(2,1)}) %all-gather.14.cloned.1.call-update) | async-done | bytes 2097168 | tf_op jit(solution)/shard_map/all_gather | solution.py:139
  125.6 3.9 %copy.48 = bf16[2048,512]{1,0:T(8,128)(2,1)} copy(bf16[2048,512]{0,1:T(8,128)(2,1)} %all-gather.14.cloned.1.call-done) | data formatting | bytes 4194304 | tf_op jit(solution)/shard_map/all_gather | solution.py:139
  129.5 5.4 %shard_map.176 = bf16[256,512]{1,0:T(8,128)(2,1)} custom-call(bf16[256,512]{1,0:T(8,128)(2,1)} %fusion.23.q_ref, bf16[8,512,256]{2,1,0:T(8,128)(2,1)} %bitcast.115, bf16[8,256,512]{2,1,0:T(8,128)(2,1)} %bitcast.116, bf16[8,512,128]{2,1,0:T(8,128)(2,1)} %pad.4.aug_ref, f32[256,1]{1,0:T(8,128)} %copy.51.gain_ref), custom_call_target="tpu_custom_call" | custom-call | flops 4294967296 | bytes 8388608 | tf_op jit(solution)/shard_map/pallas_call | solution.py:86
  134.9 23.7 %reduce-scatter.2.cloned.1.call-done = bf16[8,1,48,512]{3,2,0,1:T(8,128)(2,1)} async-done(((bf16[8,1,48,2048]{3,2,0,1:T(8,128)(2,1)}), bf16[8,1,48,512]{3,2,0,1:T(8,128)(2,1)}) %reduce-scatter.2.cloned.1.call-update) | async-done | bytes 393232 | tf_op jit(solution)/shard_map/reduce_scatter | solution.py:184
  158.6 4.6 %all-to-all-start.1 = ((bf16[8,48,512]{2,1,0:T(8,128)(2,1)}), bf16[8,48,512]{2,1,0:T(8,128)(2,1)S(1)}, u32[]{:S(2)}, u32[]{:S(2)}) async-start(bf16[8,48,512]{2,1,0:T(8,128)(2,1)} %bitcast.120), calls=%async_computation.2 | async-start | bytes 786432 | tf_op jit(solution)/shard_map/all_to_all | solution.py:186
  163.5 23.4 %all-gather.8.cloned.1.call-done = bf16[1024,512]{1,0:T(8,128)(2,1)} async-done(((bf16[256,512]{1,0:T(8,128)(2,1)}), bf16[1024,512]{1,0:T(8,128)(2,1)}) %all-gather.8.cloned.1.call-update) | async-done | bytes 1048592 | tf_op jit(solution)/shard_map/all_gather | solution.py:147
  186.8 2.8 %convolution_convert_fusion.1 = bf16[512,512]{1,0:T(8,128)(2,1)} fusion(bf16[1024,512]{1,0:T(8,128)(2,1)} %all-gather.8.cloned.1.call-done, bf16[1024,512]{1,0:T(8,128)(2,1)S(1)} %copy-done.12), kind=kOutput, calls=%fused_computation.7 | convolution fusion | flops 537133056 | bytes 2621440 | tf_op jit(solution)/shard_map/dot_general | solution.py:146
  190.3 1.3 reduce_sum.59
  (71 shorter events, 6.8 us)
Async XLA Ops:
  7.2 58.1 %copy-start = (bf16[1,256,2048]{2,1,0:T(8,128)(2,1)S(1)}, bf16[1,256,2048]{2,1,0:T(8,128)(2,1)}, u32[]{:S(2)}) copy-start(bf16[1,256,2048]{2,1,0:T(8,128)(2,1)} %param.33) | copy-start | bytes 3145732
  7.2 4.8 %copy-start.6 = (s32[128,2]{0,1:T(2,128)S(1)}, s32[128,2]{0,1:T(2,128)}, u32[]{:S(2)}) copy-start(s32[128,2]{0,1:T(2,128)} %param.29) | copy-start | bytes 3076
  7.2 3.4 %copy-start.1 = (bf16[128,2048]{1,0:T(8,128)(2,1)S(1)}, bf16[128,2048]{1,0:T(8,128)(2,1)}, u32[]{:S(2)}) copy-start(bf16[128,2048]{1,0:T(8,128)(2,1)} %param.27) | copy-start | bytes 1572868
  7.2 55.6 %all-gather.10.cloned.1.call-start = ((), (), s32[]{:S(2)}) async-start(), calls=%async_computation.4 | async-start | bytes 1966080 | tf_op jit(solution)/shard_map/all_gather | solution.py:177
  8.4 24.7 %copy-start.9 = (f32[64]{0:T(128)S(1)}, f32[64]{0:T(128)}, u32[]{:S(2)}) copy-start(f32[64]{0:T(128)} %param.23) | copy-start | bytes 772
  11.7 23.7 %copy-start.2 = (bf16[512,2048]{1,0:T(8,128)(2,1)S(1)}, bf16[512,2048]{1,0:T(8,128)(2,1)}, u32[]{:S(2)}) copy-start(bf16[512,2048]{1,0:T(8,128)(2,1)} %param.17) | copy-start | bytes 6291460
  11.7 23.7 %copy-start.13 = (f32[2048]{0:T(1024)S(1)}, f32[2048]{0:T(1024)}, u32[]{:S(2)}) copy-start(f32[2048]{0:T(1024)} %param.18) | copy-start | bytes 24580
  33.1 61.1 %all-gather.12.cloned.1.call-start = ((), (), s32[]{:S(2)}) async-start(), calls=%async_computation.6 | async-start | bytes 2359296 | tf_op jit(solution)/shard_map/all_gather | solution.py:138
  33.2 2.2 %copy-start.11 = (bf16[2048,256]{1,0:T(8,128)(2,1)S(1)}, bf16[2048,256]{1,0:T(8,128)(2,1)}, u32[]{:S(2)}) copy-start(bf16[2048,256]{1,0:T(8,128)(2,1)} %param.20) | copy-start | bytes 3145732
  37.2 88.4 %all-gather.14.cloned.1.call-start = ((), (), s32[]{:S(2)}) async-start(), calls=%async_computation.7 | async-start | bytes 2359296 | tf_op jit(solution)/shard_map/all_gather | solution.py:139
  40.0 118.6 %reduce-scatter.2.cloned.1.call-start = ((), (), s32[]{:S(2)}) async-start(), calls=%async_computation.5 | async-start | bytes 1966080 | tf_op jit(solution)/shard_map/reduce_scatter | solution.py:184
  62.8 2.4 %copy-start.4 = (bf16[8,48,2048]{2,1,0:T(8,128)(2,1)S(1)}, bf16[8,48,2048]{2,1,0:T(8,128)(2,1)}, u32[]{:S(2)}) copy-start(bf16[8,48,2048]{2,1,0:T(8,128)(2,1)} %all-gather.10.cloned.1.call-done) | copy-start | bytes 4718596
  65.3 4.3 %copy-start.10 = (f32[64]{0:T(128)S(1)}, f32[64]{0:T(128)}, u32[]{:S(2)}) copy-start(f32[64]{0:T(128)} %param.22) | copy-start | bytes 772
  65.3 4.4 %copy-start.5 = (f32[512,4]{0,1:T(4,128)S(1)}, f32[512,4]{0,1:T(4,128)}, u32[]{:S(2)}) copy-start(f32[512,4]{0,1:T(4,128)} %param.24) | copy-start | bytes 24580
  69.5 15.1 %copy-start.7 = (f32[256]{0:T(256)S(1)}, f32[256]{0:T(256)}, u32[]{:S(2)}) copy-start(f32[256]{0:T(256)} %param.25) | copy-start | bytes 3076
  69.5 117.3 %all-gather.8.cloned.1.call-start = ((), (), s32[]{:S(2)}) async-start(), calls=%async_computation.3 | async-start | bytes 1310720 | tf_op jit(solution)/shard_map/all_gather | solution.py:147
  85.4 2.0 %copy-start.3 = (bf16[512,2048]{1,0:T(8,128)(2,1)S(1)}, bf16[512,2048]{1,0:T(8,128)(2,1)}, u32[]{:S(2)}) copy-start(bf16[512,2048]{1,0:T(8,128)(2,1)} %param.17) | copy-start | bytes 6291460
  129.5 33.7 %copy-start.8 = (f32[128,2]{0,1:T(2,128)S(1)}, f32[128,2]{0,1:T(2,128)}, u32[]{:S(2)}) copy-start(f32[128,2]{0,1:T(2,128)} %param.30) | copy-start | bytes 3076
  129.5 57.3 %copy-start.12 = (bf16[1024,512]{1,0:T(8,128)(2,1)S(1)}, bf16[1024,512]{1,0:T(8,128)(2,1)}, u32[]{:S(2)}) copy-start(bf16[1024,512]{1,0:T(8,128)(2,1)} %param.26) | copy-start | bytes 3145732
  158.6 31.0 %all-to-all-start.1 = ((bf16[8,48,512]{2,1,0:T(8,128)(2,1)}), bf16[8,48,512]{2,1,0:T(8,128)(2,1)S(1)}, u32[]{:S(2)}, u32[]{:S(2)}) async-start(bf16[8,48,512]{2,1,0:T(8,128)(2,1)} %bitcast.120), calls=%async_computation.2 | async-start | bytes 786432 | tf_op jit(solution)/shard_map/all_to_all | solution.py:186
Sparse Core Ops, SparseCore 0:
  33.2 29.6 all-gather.9
  64.4 29.6 all-gather.11
  95.7 29.8 all-gather.13
  128.4 30.1 reduce-scatter.1
  160.3 26.4 all-gather.7

commit v2 on v1

--- a/solution.py
+++ b/solution.py
@@ -20,42 +20,84 @@
     return scaled * gain_vec
 
 
-def split3(x):
-    hi = lax.reduce_precision(x, 8, 7)
-    rest = x - hi
-    mid = lax.reduce_precision(rest, 8, 7)
-    return hi.astype(BF), mid.astype(BF), (rest - mid).astype(BF)
-
-
-def attend_kernel(heads, q_ref, k_ref, v_ref, aug_ref, gain_ref, o_ref, qz, m_s, l_s, acc):
+def attend_kernel(
+    heads, count, q_ref, k_ref, v_ref, g_ref, gain_ref, o_ref,
+    k_all, v_all, g_all, qz, m_s, l_s, acc, send_sem, recv_sem,
+):
     me = lax.axis_index("ep")
+    chips = count // 2
+    z = me // 2
+    c = me % 2
+    other = 2 * z + 1 - c
+    above = 2 * lax.rem(z + 1, chips) + c
+    below = 2 * lax.rem(z + chips - 1, chips) + c
     tok = q_ref.shape[1]
+    rows8 = g_ref.shape[0]
+    own = (k_ref, v_ref, g_ref)
+    slots = (k_all, v_all, g_all)
+
+    barrier = pltpu.get_barrier_semaphore()
+    for peer in (other, above, below):
+        pl.semaphore_signal(barrier, inc=1, device_id={"ep": peer}, device_id_type=pl.DeviceIdType.MESH)
+    pl.semaphore_wait(barrier, 3)
+
+    def copies(refs, src, way, dist, target):
+        return [
+            pltpu.make_async_remote_copy(
+                src_ref=refs[i],
+                dst_ref=slots[i].at[src],
+                send_sem=send_sem.at[i, way, dist],
+                recv_sem=recv_sem.at[i, src],
+                device_id={"ep": target},
+                device_id_type=pl.DeviceIdType.MESH,
+            )
+            for i in range(3)
+        ]
+
+    def held(src):
+        return [s.at[src] for s in slots]
+
+    has_up = z + 1 < chips
+
+    @pl.when(has_up)
+    def _():
+        for d in copies(own, me, 0, 0, above):
+            d.start()
+
+    @pl.when(c == 0)
+    def _():
+        for d in copies(own, me, 1, 0, other):
+            d.start()
+
     row = lax.broadcasted_iota(jnp.int32, (LANES, tok), 0)
     zeros = jnp.zeros((HD, tok), BF)
     for h in range(heads):
         q_h = q_ref[h * HD:(h + 1) * HD, :]
         parts = [q_h, zeros] if h % 2 == 0 else [zeros, q_h]
-        pick = jnp.where((row >= 3 * h) & (row < 3 * h + 3), -1.0, 0.0).astype(BF)
+        hit = (row == h) | (row == rows8 + h) | (row == 2 * rows8 + h)
+        pick = jnp.where(hit, -1.0, 0.0).astype(BF)
         qz[h] = jnp.concatenate(parts + [pick], axis=0)
 
-    def step(block, first, masked):
-        aug = aug_ref[block]
+    def step(k_blk, v_blk, g_blk, first=False):
+        g = g_blk[...]
+        hi = g.astype(BF).astype(F32)
+        rest = g - hi
+        mid = rest.astype(BF).astype(F32)
+        pad = jnp.zeros((LANES - 3 * rows8, tok), F32)
+        aug = jnp.concatenate([hi, mid, rest - mid, pad], axis=0).T.astype(BF)
         for h in range(heads):
             p = h // 2
-            keys = jnp.concatenate([k_ref[block, :, p * LANES:(p + 1) * LANES], aug], axis=1)
+            keys = jnp.concatenate([k_blk[:, p * LANES:(p + 1) * LANES], aug], axis=1)
             s = jnp.dot(keys, qz[h], preferred_element_type=F32)
-            if masked:
+            if first:
                 kpos = lax.broadcasted_iota(jnp.int32, s.shape, 0)
                 qpos = lax.broadcasted_iota(jnp.int32, s.shape, 1)
                 s = jnp.where(kpos <= qpos, s, -1e30)
             top = jnp.max(s, axis=0, keepdims=True)
-            if first:
-                new = top
-            else:
-                new = jnp.maximum(m_s[h], top)
+            new = top if first else jnp.maximum(m_s[h], top)
             e = jnp.exp(s - new)
             total = jnp.sum(e, axis=0, keepdims=True)
-            o = jnp.dot(v_ref[block, h * HD:(h + 1) * HD, :], e.astype(BF), preferred_element_type=F32)
+            o = jnp.dot(v_blk[h * HD:(h + 1) * HD, :], e.astype(BF), preferred_element_type=F32)
             if first:
                 l_s[h] = total
                 acc[h] = o
@@ -65,38 +107,89 @@
                 acc[h] = acc[h] * fix + o
             m_s[h] = new
 
-    step(me, True, True)
-
-    @pl.loop(0, me)
-    def _(i):
-        step(i, False, False)
+    step(*own, first=True)
+
+    def take(src):
+        for d in copies(held(src), src, 0, 0, other):
+            d.wait_recv()
+
+    @pl.when(c == 1)
+    def _():
+        take(other)
+        step(*held(other))
+
+    @pl.loop(1, z + 1)
+    def _(dist):
+        src = 2 * (z - dist) + c
+        take(src)
+
+        @pl.when(has_up)
+        def _():
+            for d in copies(held(src), src, 0, dist, above):
+                d.start()
+
+        for d in copies(held(src), src, 1, dist, other):
+            d.start()
+        step(*held(src))
+        src2 = 2 * (z - dist) + 1 - c
+        take(src2)
+        step(*held(src2))
 
     for h in range(heads):
         a = acc[h] / l_s[h]
         a = a * lax.rsqrt(jnp.mean(a * a, axis=0, keepdims=True) + epsilon)
         o_ref[h * HD:(h + 1) * HD, :] = (a * gain_ref[h * HD:(h + 1) * HD, :]).astype(BF)
 
-
-def attend(q_t, k_all, v_all, aug, gain):
+    @pl.when(has_up)
+    def _():
+        for d in copies(own, me, 0, 0, above):
+            d.wait_send()
+
+    @pl.when(c == 0)
+    def _():
+        for d in copies(own, me, 1, 0, other):
+            d.wait_send()
+
+    @pl.loop(1, z + 1)
+    def _(dist):
+        src = 2 * (z - dist) + c
+
+        @pl.when(has_up)
+        def _():
+            for d in copies(held(src), src, 0, dist, above):
+                d.wait_send()
+
+        for d in copies(held(src), src, 1, dist, other):
+            d.wait_send()
+
+
+def attend(q_t, k_rows, v_t, gates, gain):
     feats, tok = q_t.shape
     heads = feats // HD
+    count = lax.axis_size("ep")
     vm = pl.BlockSpec(memory_space=pltpu.VMEM)
-    blocks = k_all.shape[0]
-    scores = heads * blocks * tok * tok
+    scores = heads * count * tok * tok
     return pl.pallas_call(
-        functools.partial(attend_kernel, heads),
+        functools.partial(attend_kernel, heads, count),
         out_shape=jax.ShapeDtypeStruct((feats, tok), BF),
         in_specs=[vm] * 5,
         out_specs=vm,
         scratch_shapes=[
+            pltpu.VMEM((count,) + k_rows.shape, BF),
+            pltpu.VMEM((count,) + v_t.shape, BF),
+            pltpu.VMEM((count,) + gates.shape, F32),
             pltpu.VMEM((heads, 2 * LANES, tok), BF),
             pltpu.VMEM((heads, 1, tok), F32),
             pltpu.VMEM((heads, 1, tok), F32),
             pltpu.VMEM((heads, HD, tok), F32),
+            pltpu.SemaphoreType.DMA((3, 2, count // 2)),
+            pltpu.SemaphoreType.DMA((3, count)),
         ],
-        compiler_params=pltpu.CompilerParams(vmem_limit_bytes=56 * 1024 * 1024),
+        compiler_params=pltpu.CompilerParams(
+            vmem_limit_bytes=48 * 1024 * 1024, collective_id=1, has_side_effects=True
+        ),
         cost_estimate=pl.CostEstimate(flops=scores * 512, bytes_accessed=2**23, transcendentals=scores),
-    )(q_t, k_all, v_all, aug, gain)
+    )(q_t, k_rows, v_t, gates, gain)
 
 
 def body(
@@ -135,14 +228,9 @@
     if feats % LANES:
         k_rows = jnp.pad(k_rows, ((0, 0), (0, LANES - feats % LANES)))
     v_t = project(value_weight).astype(BF)
-    k_all = lax.all_gather(k_rows, "ep")
-    v_all = lax.all_gather(v_t, "ep")
     q_t = head_norm(project(query_weight), query_gain) * jnp.asarray(HD ** -0.5, BF)
-    gates = lax.all_gather(log_cache, "ep")
-    hi, mid, low = split3(gates)
-    aug = jnp.stack([hi, mid, low], axis=-1).reshape(gates.shape[0], tok_rows, 3 * local_heads)
-    aug = jnp.pad(aug, ((0, 0), (0, 0), (0, LANES - 3 * local_heads)))
-    head_t = attend(q_t, k_all, v_all, aug, head_gain[:, None])
+    gates = jnp.pad(jnp.transpose(log_cache), ((0, -local_heads % 8), (0, 0)))
+    head_t = attend(q_t, k_rows, v_t, gates, head_gain[:, None])
     mixer_out = lax.dot_general(
         lax.all_gather(head_t, "tp", axis=0, tiled=True),
         out_weight,

time: 199 us -> 165 us (0.83)
  waiting for transfers between devices: 101 us -> 52.9 us
  starting transfers between devices: 4.79 us -> 32.3 us
  blocking collectives: 33.1 us -> 18.8 us
  Pallas kernels: 5.39 us -> 15.9 us
  local copies, waits for them, and re-layouts: 14.6 us -> 10.1 us
  other arithmetic: 8.29 us -> 5.23 us
    all_gather x2 -> x0, waiting for transfers between devices: 31.2 us -> none  [the longest x1 27.4 us: body(): v_all = lax.all_gather(v_t, 'ep')]
    all_to_all x1, starting transfers between devices: 4.59 us -> 32.2 us  [body(): lax.all_to_all(summed.reshape(expert_count, capacity, out_cols), 'ep', sp...]
    reduce_scatter x1, waiting for transfers between devices: 23.7 us -> 1.35 us  [body(): lax.psum_scatter(partial_value.astype(BF), 'tp', scatter_dimension=3, til...]
    all_gather x1 -> x0, blocking collectives: 14.3 us -> none  [body(): gates = lax.all_gather(log_cache, 'ep')]
    pallas_call x1, Pallas kernels: 5.39 us -> 15.9 us  [attend(): pl.pallas_call(functools.partial(attend_kernel, heads, count), out_shape=...]
    all_gather x2 -> x0, local copies, waits for them, and re-layouts: 7.99 us -> none  [the longest x1 4.07 us: body(): k_all = lax.all_gather(k_rows, 'ep')]
    all_gather x1, waiting for transfers between devices: 22.8 us -> 29.7 us  [body(): piece_now = lax.all_gather(arrived, 'tp', axis=2, tiled=True)]
    mul x0 -> x3, local copies, waits for them, and re-layouts: none -> 4.98 us  [head_norm(): x = x * lax.rsqrt(jnp.mean(x * x, axis=1, keepdims=True) + epsilon)]
  transfers between devices with their start and end apart: 6 -> 4, of which waited for: 5 -> 3; matrix products, arithmetic and copies ran while one was open for 15% -> 9% of each run, Pallas kernels for 3% -> 10%
where the time goes in v2:
time: 165 us
  waiting for transfers between devices  52.9 us (32%)
  starting transfers between devices  32.3 us (20%)
  blocking collectives  18.8 us (11%)
  Pallas kernels  15.9 us (10%)
  matrix products  15.4 us (9%)
  between operations  14 us (8%)
  local copies, waits for them, and re-layouts  10.1 us (6%)
  other arithmetic  5.23 us (3%)
    all_to_all x1, starting transfers between devices, body(): lax.all_to_all(summed.reshape(expert_count, capacity, out_cols), 'ep', sp...  32.2 us
    all_gather x1, waiting for transfers between devices, body(): piece_now = lax.all_gather(arrived, 'tp', axis=2, tiled=True)  29.7 us
    all_gather x1, waiting for transfers between devices, body(): lax.all_gather(head_t, 'tp', axis=0, tiled=True)  21.8 us
    all_to_all x1, blocking collectives, body(): lax.all_to_all(share_part, 'ep', split_axis=0, concat_axis=0, tiled=True)  18.8 us
    pallas_call x1, Pallas kernels, attend(): pl.pallas_call(functools.partial(attend_kernel, heads, count), out_shape=...  15.9 us
    mul x3, local copies, waits for them, and re-layouts, head_norm(): x = x * lax.rsqrt(jnp.mean(x * x, axis=1, keepdims=True) + epsilon)  4.98 us
    dot_general x3, matrix products, project(): lax.dot_general(weight, normed, (((0,), (1,)), ((), ())), preferred_eleme...  4.94 us
    dot_general x1, matrix products, body(): jnp.einsum('sjcf,jfd->sjcd', hidden, expert_down, preferred_element_type=...  4.8 us
  transfers between devices with their start and end apart: 4, of which 3 were waited for; matrix products, arithmetic and copies ran while one was open for 9% of the time, Pallas kernels for 10%

profile of v2, /device:TPU:0, one launch (start us, length us, event | category | flops | bytes accessed | tf_op | source)
XLA Modules:
  0.0 164.7 jit_solution(14626212331498446881)
XLA Ops:
  7.2 0.9 copy.47
  8.4 1.1 convert_element_type.66
  9.8 0.6 reduce-window.6
  11.0 0.8 dynamic-slice
  12.1 18.8 %all_to_all.10 = bf16[8,48,512]{2,1,0:T(8,128)(2,1)} all-to-all(bf16[8,48,512]{2,1,0:T(8,128)(2,1)S(1)} %bitcast.87), channel_id=1, replica_groups=mesh['ep'=8,'tp'=4] {'ep'}, dimensions={0} | all-to-all | bytes 786432 | tf_op jit(solution)/shard_map/all_to_all | solution.py:264
  31.0 29.7 %all-gather.5.cloned.1.call-done = bf16[8,48,2048]{2,1,0:T(8,128)(2,1)} async-done(((bf16[8,48,512]{2,1,0:T(8,128)(2,1)}), bf16[8,48,2048]{2,1,0:T(8,128)(2,1)}) %all-gather.5.cloned.1.call-update) | async-done | bytes 1572880 | tf_op jit(solution)/shard_map/all_gather | solution.py:265
  60.7 2.3 %convolution_bitcast_fusion.3 = f32[8,1,48,256]{3,2,0,1:T(8,128)S(1)} fusion(bf16[8,48,2048]{2,1,0:T(8,128)(2,1)} %all-gather.5.cloned.1.call-done, bf16[1,2048,256]{2,1,0:T(8,128)(2,1)} %param.31), kind=kOutput, calls=%fused_computation.14 | convolution fusion | flops 402653184 | bytes 3014656 | tf_op jit(solution)/shard_map/sjcd,jdf->sjcf/dot_general | solution.py:268
  63.0 4.8 %fusion.3 = bf16[8,1,48,2048]{3,2,0,1:T(8,128)(2,1)} fusion(bf16[1,256,2048]{2,1,0:T(8,128)(2,1)S(1)} %copy-done, bf16[8,48,2048]{2,1,0:T(8,128)(2,1)} %all-gather.5.cloned.1.call-done, bf16[1,2048,256]{2,1,0:T(8,128)(2,1)} %param.32, f32[8,1,48,256]{3,2,0,1:T(8,128)S(1)} %convolution_bitcast_fusion.3), kind=kOutput, calls=%fused_computation.6 | convolution fusion | flops 806682624 | bytes 5636096 | tf_op jit(solution)/shard_map/sjcf,jfd->sjcd/dot_general | solution.py:271
  67.9 0.5 fusion
  68.5 0.6 copy-done.11
  69.2 1.7 %fusion.37 = (f32[256,512]{0,1:T(8,128)}, f32[256,512]{0,1:T(8,128)}) fusion(bf16[2048,256]{1,0:T(8,128)(2,1)S(1)} %copy-done.11, bf16[512,2048]{1,0:T(8,128)(2,1)S(1)} %copy-done.2, f32[2048]{0:T(1024)S(1)} %copy-done.14, f32[512]{0:T(512)S(1)} %add_rsqrt_fusion.2), kind=kOutput, calls=%fused_computation.61 | convolution fusion | flops 541196288 | bytes 4204544 | tf_op jit(solution)/shard_map/dot_general | solution.py:220
  70.9 2.1 %copy.43 = f32[256,512]{1,0:T(8,128)} copy(f32[256,512]{0,1:T(8,128)} %get-tuple-element.6) | data formatting | bytes 1048576 | tf_op jit(solution)/shard_map/mul | solution.py:224
  73.0 1.1 bitcast_reduce_fusion
  74.1 0.9 mul.161
  75.0 2.0 %copy.44 = f32[256,512]{0,1:T(8,128)} copy(f32[256,512]{1,0:T(8,128)} %bitcast.85) | data formatting | bytes 1048576 | tf_op jit(solution)/shard_map/mul | solution.py:224
  77.4 2.3 %bitcast_reduce_fusion.1 = (f32[4,512]{1,0:T(4,128)S(1)}, f32[256,512]{1,0:T(8,128)S(1)}) fusion(bf16[2048,256]{1,0:T(8,128)(2,1)} %param.19, bf16[512,2048]{1,0:T(8,128)(2,1)S(1)} %copy-done.2, f32[2048]{0:T(1024)S(1)} %copy-done.14, f32[512]{0:T(512)S(1)} %add_rsqrt_fusion.2), kind=kOutput, calls=%fused_computation.27 | convolution fusion | flops 541325312 | bytes 3688448 | tf_op jit(solution)/shard_map/dot_general | solution.py:220
  79.9 1.0 copy-done.12
  80.9 1.0 fusion.6.v_ref
  81.9 15.9 %shard_map.176 = bf16[256,512]{1,0:T(8,128)(2,1)} custom-call(bf16[256,512]{1,0:T(8,128)(2,1)S(1)} %fusion.22.q_ref, bf16[512,256]{1,0:T(8,128)(2,1)S(1)} %fusion.21.k_ref, bf16[256,512]{1,0:T(8,128)(2,1)S(1)} %fusion.6.v_ref, f32[8,512]{1,0:T(8,128)S(1)} %pad.4.g_ref, f32[256,1]{1,0:T(8,128)S(1)} %copy.46.gain_ref), custom_call_target="tpu_custom_call" | custom-call | flops 4294967296 | bytes 8388608 | tf_op jit(solution)/shard_map/pallas_call | solution.py:172
  97.8 1.4 reduce-scatter.2.cloned.1.call-done
  99.2 32.2 %all-to-all-start.1 = ((bf16[8,48,512]{2,1,0:T(8,128)(2,1)}), bf16[8,48,512]{2,1,0:T(8,128)(2,1)S(1)}, u32[]{:S(2)}, u32[]{:S(2)}) async-start(bf16[8,48,512]{2,1,0:T(8,128)(2,1)} %bitcast.88), calls=%async_computation.2 | async-start | bytes 786432 | tf_op jit(solution)/shard_map/all_to_all | solution.py:274
  131.6 21.8 %all-gather.3.cloned.1.call-done = bf16[1024,512]{1,0:T(8,128)(2,1)} async-done(((bf16[256,512]{1,0:T(8,128)(2,1)}), bf16[1024,512]{1,0:T(8,128)(2,1)}) %all-gather.3.cloned.1.call-update) | async-done | bytes 1048592 | tf_op jit(solution)/shard_map/all_gather | solution.py:235
  153.4 2.8 %convolution_convert_fusion.1 = bf16[512,512]{1,0:T(8,128)(2,1)} fusion(bf16[1024,512]{1,0:T(8,128)(2,1)} %all-gather.3.cloned.1.call-done, bf16[1024,512]{1,0:T(8,128)(2,1)S(1)} %copy-done.13), kind=kOutput, calls=%fused_computation.7 | convolution fusion | flops 537133056 | bytes 2621440 | tf_op jit(solution)/shard_map/dot_general | solution.py:234
  156.8 1.3 reduce_sum.59
  (65 shorter events, 3.2 us)
Async XLA Ops:
  7.2 55.9 %copy-start = (bf16[1,256,2048]{2,1,0:T(8,128)(2,1)S(1)}, bf16[1,256,2048]{2,1,0:T(8,128)(2,1)}, u32[]{:S(2)}) copy-start(bf16[1,256,2048]{2,1,0:T(8,128)(2,1)} %param.33) | copy-start | bytes 3145732
  7.2 3.8 %copy-start.6 = (s32[128,2]{0,1:T(2,128)S(1)}, s32[128,2]{0,1:T(2,128)}, u32[]{:S(2)}) copy-start(s32[128,2]{0,1:T(2,128)} %param.29) | copy-start | bytes 3076
  7.2 2.4 %copy-start.1 = (bf16[128,2048]{1,0:T(8,128)(2,1)S(1)}, bf16[128,2048]{1,0:T(8,128)(2,1)}, u32[]{:S(2)}) copy-start(bf16[128,2048]{1,0:T(8,128)(2,1)} %param.27) | copy-start | bytes 1572868
  7.2 53.5 %all-gather.5.cloned.1.call-start = ((), (), s32[]{:S(2)}) async-start(), calls=%async_computation.4 | async-start | bytes 1966080 | tf_op jit(solution)/shard_map/all_gather | solution.py:265
  30.9 68.2 %reduce-scatter.2.cloned.1.call-start = ((), (), s32[]{:S(2)}) async-start(), calls=%async_computation.5 | async-start | bytes 1966080 | tf_op jit(solution)/shard_map/reduce_scatter | solution.py:272
  63.0 4.9 %copy-start.2 = (bf16[512,2048]{1,0:T(8,128)(2,1)S(1)}, bf16[512,2048]{1,0:T(8,128)(2,1)}, u32[]{:S(2)}) copy-start(bf16[512,2048]{1,0:T(8,128)(2,1)} %param.17) | copy-start | bytes 6291460
  67.8 0.7 copy-start.14
  67.9 85.5 %all-gather.3.cloned.1.call-start = ((), (), s32[]{:S(2)}) async-start(), calls=%async_computation.3 | async-start | bytes 1310720 | tf_op jit(solution)/shard_map/all_gather | solution.py:235
  67.9 1.2 copy-start.11
  70.9 6.1 %copy-start.9 = (f32[64]{0:T(128)S(1)}, f32[64]{0:T(128)}, u32[]{:S(2)}) copy-start(f32[64]{0:T(128)} %param.23) | copy-start | bytes 772
  70.9 6.2 %copy-start.10 = (f32[64]{0:T(128)S(1)}, f32[64]{0:T(128)}, u32[]{:S(2)}) copy-start(f32[64]{0:T(128)} %param.22) | copy-start | bytes 772
  70.9 6.3 %copy-start.7 = (f32[256]{0:T(256)S(1)}, f32[256]{0:T(256)}, u32[]{:S(2)}) copy-start(f32[256]{0:T(256)} %param.25) | copy-start | bytes 3076
  70.9 6.4 %copy-start.5 = (f32[512,4]{0,1:T(4,128)S(1)}, f32[512,4]{0,1:T(4,128)}, u32[]{:S(2)}) copy-start(f32[512,4]{0,1:T(4,128)} %param.24) | copy-start | bytes 24580
  77.3 2.4 %copy-start.3 = (f32[256,512]{0,1:T(8,128)S(1)}, f32[256,512]{0,1:T(8,128)}, u32[]{:S(2)}) copy-start(f32[256,512]{0,1:T(8,128)} %copy.44) | copy-start | bytes 1572868
  77.3 2.4 %copy-start.4 = (f32[256,512]{0,1:T(8,128)S(1)}, f32[256,512]{0,1:T(8,128)}, u32[]{:S(2)}) copy-start(f32[256,512]{0,1:T(8,128)} %get-tuple-element.7) | copy-start | bytes 1572868
  79.6 1.3 copy-start.12
  81.9 49.5 %copy-start.8 = (f32[128,2]{0,1:T(2,128)S(1)}, f32[128,2]{0,1:T(2,128)}, u32[]{:S(2)}) copy-start(f32[128,2]{0,1:T(2,128)} %param.30) | copy-start | bytes 3076
  81.9 71.5 %copy-start.13 = (bf16[1024,512]{1,0:T(8,128)(2,1)S(1)}, bf16[1024,512]{1,0:T(8,128)(2,1)}, u32[]{:S(2)}) copy-start(bf16[1024,512]{1,0:T(8,128)(2,1)} %param.26) | copy-start | bytes 3145732
  99.2 57.0 %all-to-all-start.1 = ((bf16[8,48,512]{2,1,0:T(8,128)(2,1)}), bf16[8,48,512]{2,1,0:T(8,128)(2,1)S(1)}, u32[]{:S(2)}, u32[]{:S(2)}) async-start(bf16[8,48,512]{2,1,0:T(8,128)(2,1)} %bitcast.88), calls=%async_computation.2 | async-start | bytes 786432 | tf_op jit(solution)/shard_map/all_to_all | solution.py:274
Sparse Core Ops, SparseCore 0:
  31.1 29.6 all-gather.4
  68.0 31.1 reduce-scatter.1
  101.0 52.3 all-gather.2

commit v3 on v2

--- a/solution.py
+++ b/solution.py
@@ -135,10 +135,14 @@
         take(src2)
         step(*held(src2))
 
+    outs = []
     for h in range(heads):
         a = acc[h] / l_s[h]
         a = a * lax.rsqrt(jnp.mean(a * a, axis=0, keepdims=True) + epsilon)
-        o_ref[h * HD:(h + 1) * HD, :] = (a * gain_ref[h * HD:(h + 1) * HD, :]).astype(BF)
+        outs.append(a * gain_ref[h * HD:(h + 1) * HD, :])
+    if heads * HD % LANES:
+        outs.append(jnp.zeros((LANES - heads * HD % LANES, tok), F32))
+    o_ref[...] = jnp.concatenate(outs, axis=0).T.astype(BF)
 
     @pl.when(has_up)
     def _():
@@ -171,7 +175,7 @@
     scores = heads * count * tok * tok
     return pl.pallas_call(
         functools.partial(attend_kernel, heads, count),
-        out_shape=jax.ShapeDtypeStruct((feats, tok), BF),
+        out_shape=jax.ShapeDtypeStruct((tok, feats + -feats % LANES), BF),
         in_specs=[vm] * 5,
         out_specs=vm,
         scratch_shapes=[
@@ -190,6 +194,92 @@
         ),
         cost_estimate=pl.CostEstimate(flops=scores * 512, bytes_accessed=2**23, transcendentals=scores),
     )(q_t, k_rows, v_t, gates, gain)
+
+
+def tail_kernel(
+    ep_count, tp_count, feats, head_ref, w_ref, back_ref, o_ref, ret_ref,
+    heads_in, rows_in, total, ep_send, ep_recv, tp_send, tp_recv,
+):
+    ep = lax.axis_index("ep")
+    tp = lax.axis_index("tp")
+    mesh_ids = pl.DeviceIdType.MESH
+    barrier = pltpu.get_barrier_semaphore()
+    for d in range(1, tp_count):
+        pl.semaphore_signal(barrier, inc=1, device_id={"tp": lax.rem(tp + d, tp_count)}, device_id_type=mesh_ids)
+    for d in range(1, ep_count):
+        pl.semaphore_signal(barrier, inc=1, device_id={"ep": lax.rem(ep + d, ep_count)}, device_id_type=mesh_ids)
+    pl.semaphore_wait(barrier, ep_count + tp_count - 2)
+
+    def head_copy(d):
+        return pltpu.make_async_remote_copy(
+            src_ref=head_ref,
+            dst_ref=heads_in.at[d],
+            send_sem=tp_send.at[d],
+            recv_sem=tp_recv.at[d],
+            device_id={"tp": lax.rem(tp + d, tp_count)},
+            device_id_type=mesh_ids,
+        )
+
+    def row_copy(d):
+        peer = lax.rem(ep + d, ep_count)
+        return pltpu.make_async_remote_copy(
+            src_ref=back_ref.at[peer],
+            dst_ref=rows_in.at[d],
+            send_sem=ep_send.at[d],
+            recv_sem=ep_recv.at[d],
+            device_id={"ep": peer},
+            device_id_type=mesh_ids,
+        )
+
+    for d in range(1, tp_count):
+        head_copy(d).start()
+    for d in range(1, ep_count):
+        row_copy(d).start()
+
+    def part(block, owner):
+        w = w_ref[pl.ds(pl.multiple_of(owner * feats, feats), feats), :]
+        return jnp.dot(block[:, :feats], w, preferred_element_type=F32)
+
+    total[...] = part(head_ref[...], tp)
+    ret_ref[ep] = back_ref[ep]
+    for d in range(1, tp_count):
+        head_copy(d).wait_recv()
+        total[...] += part(heads_in[d], lax.rem(tp + tp_count - d, tp_count))
+    o_ref[...] = total[...].astype(BF)
+    for d in range(1, ep_count):
+        row_copy(d).wait_recv()
+        ret_ref[lax.rem(ep + ep_count - d, ep_count)] = rows_in[d]
+    for d in range(1, tp_count):
+        head_copy(d).wait_send()
+    for d in range(1, ep_count):
+        row_copy(d).wait_send()
+
+
+def tail(head, weight, back):
+    ep_count = lax.axis_size("ep")
+    tp_count = lax.axis_size("tp")
+    feats = weight.shape[0] // tp_count
+    vm = pl.BlockSpec(memory_space=pltpu.VMEM)
+    out = (head.shape[0], weight.shape[1])
+    return pl.pallas_call(
+        functools.partial(tail_kernel, ep_count, tp_count, feats),
+        out_shape=(jax.ShapeDtypeStruct(out, BF), jax.ShapeDtypeStruct(back.shape, BF)),
+        in_specs=[vm] * 3,
+        out_specs=(vm, vm),
+        scratch_shapes=[
+            pltpu.VMEM((tp_count,) + head.shape, BF),
+            pltpu.VMEM(back.shape, BF),
+            pltpu.VMEM(out, F32),
+            pltpu.SemaphoreType.DMA((ep_count,)),
+            pltpu.SemaphoreType.DMA((ep_count,)),
+            pltpu.SemaphoreType.DMA((tp_count,)),
+            pltpu.SemaphoreType.DMA((tp_count,)),
+        ],
+        compiler_params=pltpu.CompilerParams(
+            vmem_limit_bytes=32 * 1024 * 1024, collective_id=2, has_side_effects=True
+        ),
+        cost_estimate=pl.CostEstimate(flops=2**30, bytes_accessed=2**22, transcendentals=0),
+    )(head, weight, back)
 
 
 def body(
@@ -230,14 +320,6 @@
     v_t = project(value_weight).astype(BF)
     q_t = head_norm(project(query_weight), query_gain) * jnp.asarray(HD ** -0.5, BF)
     gates = jnp.pad(jnp.transpose(log_cache), ((0, -local_heads % 8), (0, 0)))
-    head_t = attend(q_t, k_rows, v_t, gates, head_gain[:, None])
-    mixer_out = lax.dot_general(
-        lax.all_gather(head_t, "tp", axis=0, tiled=True),
-        out_weight,
-        (((0,), (0,)), ((), ())),
-        preferred_element_type=F32,
-    ).astype(BF)
-
     moe_rows = moe_in.shape[0]
     top_count = routes.shape[1]
     local_experts = expert_gate.shape[0]
@@ -263,21 +345,18 @@
     )
     arrived = lax.all_to_all(share_part, "ep", split_axis=0, concat_axis=0, tiled=True)
     piece_now = lax.all_gather(arrived, "tp", axis=2, tiled=True)
+    piece_now, q_t, k_rows, v_t = lax.optimization_barrier((piece_now, q_t, k_rows, v_t))
     piece_cols = piece_now.shape[2]
     piece_rows = piece_now.reshape(senders, local_experts, capacity, piece_cols)
     gate_next = jnp.einsum("sjcd,jdf->sjcf", piece_rows, expert_gate, preferred_element_type=F32)
     up_next = jnp.einsum("sjcd,jdf->sjcf", piece_rows, expert_up, preferred_element_type=F32)
     hidden = (jax.nn.silu(gate_next) * up_next).astype(BF)
     partial_value = jnp.einsum("sjcf,jfd->sjcd", hidden, expert_down, preferred_element_type=F32)
-    summed = lax.psum_scatter(partial_value.astype(BF), "tp", scatter_dimension=3, tiled=True)
+    partial_value, q_t = lax.optimization_barrier((partial_value.astype(BF), q_t))
+    summed = lax.psum_scatter(partial_value, "tp", scatter_dimension=3, tiled=True)
     out_cols = summed.shape[3]
-    returned = lax.all_to_all(
-        summed.reshape(expert_count, capacity, out_cols),
-        "ep",
-        split_axis=0,
-        concat_axis=0,
-        tiled=True,
-    )
+    head = attend(q_t, k_rows, v_t, gates, head_gain[:, None])
+    mixer_out, returned = tail(head, out_weight, summed.reshape(expert_count, capacity, out_cols))
     flat = returned.reshape(expert_count * capacity, out_cols)
     pick = (slot_index[:, None] == slots[None, :]).astype(BF)
     picked = jnp.dot(pick, flat, preferred_element_type=F32)

time: 165 us -> 144 us (0.87)
  starting transfers between devices: 32.3 us -> 0.08 us
  Pallas kernels: 15.9 us -> 46.3 us
  waiting for transfers between devices: 52.9 us -> 30.4 us
  other arithmetic: 5.23 us -> 7.94 us
    all_to_all x1 -> x0, starting transfers between devices: 32.2 us -> none  [body(): lax.all_to_all(summed.reshape(expert_count, capacity, out_cols), 'ep', sp...]
    pallas_call x0 -> x1, Pallas kernels: none -> 31.1 us  [tail(): pl.pallas_call(functools.partial(tail_kernel, ep_count, tp_count, feats),...]
    all_gather x1 -> x0, waiting for transfers between devices: 21.8 us -> none  [body(): lax.all_gather(head_t, 'tp', axis=0, tiled=True)]
    all_gather x1, waiting for transfers between devices: 29.7 us -> 14.7 us  [body(): piece_now = lax.all_gather(arrived, 'tp', axis=2, tiled=True)]
    reduce_scatter x1, waiting for transfers between devices: 1.35 us -> 15.7 us  [body(): lax.psum_scatter(partial_value, 'tp', scatter_dimension=3, tiled=True)]
    dot_general x1 -> x0, matrix products: 2.76 us -> none  [body(): lax.dot_general(lax.all_gather(head_t, 'tp', axis=0, tiled=True), out_wei...]
    reduce_sum x2, other arithmetic: 0.67 us -> 2.35 us  [row_norm(): jnp.mean(floats * floats, axis=-1, keepdims=True) + epsilon]
    unnamed x32 -> x39, local copies, waits for them, and re-layouts: 2.86 us -> 4.23 us
  transfers between devices with their start and end apart: 4 -> 2, of which waited for: 3 -> 2; matrix products, arithmetic and copies ran while one was open for 9% -> 10% of each run, Pallas kernels for 10% -> 11%
where the time goes in v3:
time: 144 us; the launch traced here: 143 us
  Pallas kernels  46.3 us (32%)
  waiting for transfers between devices  30.4 us (21%)
  blocking collectives  18.8 us (13%)
  between operations  14.3 us (10%)
  matrix products  14 us (10%)
  local copies, waits for them, and re-layouts  11.6 us (8%)
  other arithmetic  7.94 us (6%)
    pallas_call x1, Pallas kernels, tail(): pl.pallas_call(functools.partial(tail_kernel, ep_count, tp_count, feats),...  31.1 us
    all_to_all x1, blocking collectives, body(): lax.all_to_all(share_part, 'ep', split_axis=0, concat_axis=0, tiled=True)  18.8 us
    reduce_scatter x1, waiting for transfers between devices, body(): lax.psum_scatter(partial_value, 'tp', scatter_dimension=3, tiled=True)  15.7 us
    pallas_call x1, Pallas kernels, attend(): pl.pallas_call(functools.partial(attend_kernel, heads, count), out_shape=...  15.2 us
    all_gather x1, waiting for transfers between devices, body(): piece_now = lax.all_gather(arrived, 'tp', axis=2, tiled=True)  14.7 us
    dot_general x3, matrix products, project(): lax.dot_general(weight, normed, (((0,), (1,)), ((), ())), preferred_eleme...  4.98 us
    mul x3, local copies, waits for them, and re-layouts, head_norm(): x = x * lax.rsqrt(jnp.mean(x * x, axis=1, keepdims=True) + epsilon)  4.96 us
    dot_general x1, matrix products, body(): jnp.einsum('sjcf,jfd->sjcd', hidden, expert_down, preferred_element_type=...  4.28 us
  transfers between devices with their start and end apart: 2, of which 2 were waited for; matrix products, arithmetic and copies ran while one was open for 10% of the time, Pallas kernels for 11%

profile of v3, /device:TPU:0, one launch (start us, length us, event | category | flops | bytes accessed | tf_op | source)
XLA Modules:
  0.0 143.4 jit_solution(6104183552854667356)
XLA Ops:
  7.2 0.9 copy.44
  8.4 2.1 %convert_element_type.57 = f32[128,2048]{1,0:T(8,128)} convert(bf16[128,2048]{1,0:T(8,128)(2,1)} %param.27) | non-fusion elementwise | flops 262144 | bytes 1572864 | tf_op jit(solution)/shard_map/convert_element_type | solution.py:18
  10.8 0.6 reduce-window.6
  12.0 0.9 dynamic-slice
  13.0 1.3 convolution_convert_fusion.1
  14.3 18.8 %all_to_all.5 = bf16[8,48,512]{2,1,0:T(8,128)(2,1)} all-to-all(bf16[8,48,512]{2,1,0:T(8,128)(2,1)S(1)} %bitcast.86), channel_id=1, replica_groups=mesh['ep'=8,'tp'=4] {'ep'}, dimensions={0} | all-to-all | bytes 786432 | tf_op jit(solution)/shard_map/all_to_all | solution.py:346
  33.1 2.2 %fusion = f32[512]{0:T(512)S(1)} fusion(bf16[512,2048]{1,0:T(8,128)(2,1)} %param.17), kind=kLoop, calls=%fused_computation.2 | loop fusion | flops 3145216 | bytes 2099200 | tf_op jit(solution)/shard_map/reduce_sum | solution.py:19
  35.3 1.7 %fusion.37 = (f32[256,512]{0,1:T(8,128)}, f32[256,512]{0,1:T(8,128)}) fusion(bf16[2048,256]{1,0:T(8,128)(2,1)S(1)} %copy-done.15, bf16[512,2048]{1,0:T(8,128)(2,1)S(1)} %copy-done.4, f32[2048]{0:T(1024)S(1)} %copy-done.17, f32[512]{0:T(512)S(1)} %add_rsqrt_fusion.2), kind=kOutput, calls=%fused_computation.60 | convolution fusion | flops 541196288 | bytes 4204544 | tf_op jit(solution)/shard_map/dot_general | solution.py:310
  37.0 2.1 %copy.48 = f32[256,512]{1,0:T(8,128)} copy(f32[256,512]{0,1:T(8,128)} %get-tuple-element.22) | data formatting | bytes 1048576 | tf_op jit(solution)/shard_map/mul | solution.py:314
  39.1 1.1 bitcast_reduce_fusion
  40.2 0.9 mul.170
  41.1 2.0 %copy.49 = f32[256,512]{0,1:T(8,128)} copy(f32[256,512]{1,0:T(8,128)} %bitcast.85) | data formatting | bytes 1048576 | tf_op jit(solution)/shard_map/mul | solution.py:314
  43.3 2.3 %bitcast_reduce_fusion.1 = (f32[4,512]{1,0:T(4,128)S(1)}, f32[256,512]{1,0:T(8,128)S(1)}) fusion(bf16[2048,256]{1,0:T(8,128)(2,1)} %param.19, bf16[512,2048]{1,0:T(8,128)(2,1)S(1)} %copy-done.4, f32[2048]{0:T(1024)S(1)} %copy-done.17, f32[512]{0:T(512)S(1)} %add_rsqrt_fusion.2), kind=kOutput, calls=%fused_computation.26 | convolution fusion | flops 541325312 | bytes 3688448 | tf_op jit(solution)/shard_map/dot_general | solution.py:310
  45.9 1.3 copy-done.5
  47.2 1.0 fusion.6.v_ref
  48.2 14.7 %all-gather.2.cloned.1.call-done = bf16[8,48,2048]{2,1,0:T(8,128)(2,1)} async-done(((bf16[8,48,512]{2,1,0:T(8,128)(2,1)}), bf16[8,48,2048]{2,1,0:T(8,128)(2,1)}) %all-gather.2.cloned.1.call-update) | async-done | bytes 1572880 | tf_op jit(solution)/shard_map/all_gather | solution.py:347
  62.9 3.1 %convolution_bitcast_fusion.3 = f32[8,1,48,256]{3,2,0,1:T(8,128)} fusion(bf16[8,48,2048]{2,1,0:T(8,128)(2,1)} %all-gather.2.cloned.1.call-done, bf16[1,2048,256]{2,1,0:T(8,128)(2,1)} %param.31), kind=kOutput, calls=%fused_computation.13 | convolution fusion | flops 402653184 | bytes 3014656 | tf_op jit(solution)/shard_map/sjcd,jdf->sjcf/dot_general | solution.py:351
  66.0 4.3 %fusion.3 = bf16[8,1,48,2048]{3,2,0,1:T(8,128)(2,1)} fusion(bf16[1,256,2048]{2,1,0:T(8,128)(2,1)S(1)} %copy-done, bf16[8,48,2048]{2,1,0:T(8,128)(2,1)S(1)} %copy-done.7, bf16[1,2048,256]{2,1,0:T(8,128)(2,1)} %param.32, f32[8,1,48,256]{3,2,0,1:T(8,128)} %convolution_bitcast_fusion.3), kind=kOutput, calls=%fused_computation.6 | convolution fusion | flops 806682624 | bytes 5636096 | tf_op jit(solution)/shard_map/sjcf,jfd->sjcd/dot_general | solution.py:354
  70.8 15.2 %shard_map.176.head_ref = bf16[512,256]{1,0:T(8,128)(2,1)S(1)} custom-call(bf16[256,512]{1,0:T(8,128)(2,1)S(1)} %fusion.22.q_ref, bf16[512,256]{1,0:T(8,128)(2,1)S(1)} %fusion.21.k_ref, bf16[256,512]{1,0:T(8,128)(2,1)S(1)} %fusion.6.v_ref, f32[8,512]{1,0:T(8,128)S(1)} %pad.4.g_ref, f32[256,1]{1,0:T(8,128)S(1)} %copy.51.gain_ref), custom_call_target="tpu_custom_call" | custom-call | flops 4294967296 | bytes 8388608 | tf_op jit(solution)/shard_map/pallas_call | solution.py:176
  86.0 15.7 %reduce-scatter.2.cloned.1.call-done = bf16[8,1,48,512]{3,2,0,1:T(8,128)(2,1)} async-done(((bf16[8,1,48,2048]{3,2,0,1:T(8,128)(2,1)}), bf16[8,1,48,512]{3,2,0,1:T(8,128)(2,1)}) %reduce-scatter.2.cloned.1.call-update) | async-done | bytes 393232 | tf_op jit(solution)/shard_map/reduce_scatter | solution.py:356
  101.7 1.0 copy-done.2
  102.6 31.1 %shard_map.177 = (bf16[512,512]{1,0:T(8,128)(2,1)S(1)}, bf16[8,48,512]{2,1,0:T(8,128)(2,1)S(1)}) custom-call(bf16[512,256]{1,0:T(8,128)(2,1)S(1)} %shard_map.176.head_ref, bf16[1024,512]{1,0:T(8,128)(2,1)S(1)} %copy-done.1, bf16[8,48,512]{2,1,0:T(8,128)(2,1)S(1)} %bitcast.84), custom_call_target="tpu_custom_call" | custom-call | flops 1073741824 | bytes 4194304 | tf_op jit(solution)/shard_map/pallas_call | solution.py:264
  134.4 1.3 reduce_sum.59
  135.7 0.8 copy.56
  (67 shorter events, 2.7 us)
Async XLA Ops:
  7.2 58.8 %copy-start = (bf16[1,256,2048]{2,1,0:T(8,128)(2,1)S(1)}, bf16[1,256,2048]{2,1,0:T(8,128)(2,1)}, u32[]{:S(2)}) copy-start(bf16[1,256,2048]{2,1,0:T(8,128)(2,1)} %param.33) | copy-start | bytes 3145732
  7.2 4.8 %copy-start.10 = (s32[128,2]{0,1:T(2,128)S(1)}, s32[128,2]{0,1:T(2,128)}, u32[]{:S(2)}) copy-start(s32[128,2]{0,1:T(2,128)} %param.29) | copy-start | bytes 3076
  7.2 3.4 %copy-start.3 = (bf16[128,2048]{1,0:T(8,128)(2,1)S(1)}, bf16[128,2048]{1,0:T(8,128)(2,1)}, u32[]{:S(2)}) copy-start(bf16[128,2048]{1,0:T(8,128)(2,1)} %param.27) | copy-start | bytes 1572868
  7.2 55.7 %all-gather.2.cloned.1.call-start = ((), (), s32[]{:S(2)}) async-start(), calls=%async_computation.2 | async-start | bytes 1966080 | tf_op jit(solution)/shard_map/all_gather | solution.py:347
  11.7 23.6 %copy-start.4 = (bf16[512,2048]{1,0:T(8,128)(2,1)S(1)}, bf16[512,2048]{1,0:T(8,128)(2,1)}, u32[]{:S(2)}) copy-start(bf16[512,2048]{1,0:T(8,128)(2,1)} %param.17) | copy-start | bytes 6291460
  11.7 23.6 %copy-start.17 = (f32[2048]{0:T(1024)S(1)}, f32[2048]{0:T(1024)}, u32[]{:S(2)}) copy-start(f32[2048]{0:T(1024)} %param.18) | copy-start | bytes 24580
  33.1 68.6 %reduce-scatter.2.cloned.1.call-start = ((), (), s32[]{:S(2)}) async-start(), calls=%async_computation.3 | async-start | bytes 1966080 | tf_op jit(solution)/shard_map/reduce_scatter | solution.py:356
  33.1 2.2 %copy-start.15 = (bf16[2048,256]{1,0:T(8,128)(2,1)S(1)}, bf16[2048,256]{1,0:T(8,128)(2,1)}, u32[]{:S(2)}) copy-start(bf16[2048,256]{1,0:T(8,128)(2,1)} %param.20) | copy-start | bytes 3145732
  37.0 6.1 %copy-start.13 = (f32[64]{0:T(128)S(1)}, f32[64]{0:T(128)}, u32[]{:S(2)}) copy-start(f32[64]{0:T(128)} %param.23) | copy-start | bytes 772
  37.0 6.2 %copy-start.14 = (f32[64]{0:T(128)S(1)}, f32[64]{0:T(128)}, u32[]{:S(2)}) copy-start(f32[64]{0:T(128)} %param.22) | copy-start | bytes 772
  43.3 2.5 %copy-start.6 = (f32[256,512]{0,1:T(8,128)S(1)}, f32[256,512]{0,1:T(8,128)}, u32[]{:S(2)}) copy-start(f32[256,512]{0,1:T(8,128)} %copy.49) | copy-start | bytes 1572868
  43.3 2.5 %copy-start.8 = (f32[256,512]{0,1:T(8,128)S(1)}, f32[256,512]{0,1:T(8,128)}, u32[]{:S(2)}) copy-start(f32[256,512]{0,1:T(8,128)} %get-tuple-element.23) | copy-start | bytes 1572868
  43.3 2.6 %copy-start.16 = (bf16[2048,256]{1,0:T(8,128)(2,1)S(1)}, bf16[2048,256]{1,0:T(8,128)(2,1)}, u32[]{:S(2)}) copy-start(bf16[2048,256]{1,0:T(8,128)(2,1)} %param.21) | copy-start | bytes 3145732
  45.6 1.6 %copy-start.5 = (bf16[512,2048]{1,0:T(8,128)(2,1)S(1)}, bf16[512,2048]{1,0:T(8,128)(2,1)}, u32[]{:S(2)}) copy-start(bf16[512,2048]{1,0:T(8,128)(2,1)} %param.17) | copy-start | bytes 6291460
  62.9 3.1 %copy-start.7 = (bf16[8,48,2048]{2,1,0:T(8,128)(2,1)S(1)}, bf16[8,48,2048]{2,1,0:T(8,128)(2,1)}, u32[]{:S(2)}) copy-start(bf16[8,48,2048]{2,1,0:T(8,128)(2,1)} %all-gather.2.cloned.1.call-done) | copy-start | bytes 4718596
  66.0 4.3 %copy-start.11 = (f32[256]{0:T(256)S(1)}, f32[256]{0:T(256)}, u32[]{:S(2)}) copy-start(f32[256]{0:T(256)} %param.25) | copy-start | bytes 3076
  66.0 4.5 %copy-start.12 = (f32[128,2]{0,1:T(2,128)S(1)}, f32[128,2]{0,1:T(2,128)}, u32[]{:S(2)}) copy-start(f32[128,2]{0,1:T(2,128)} %param.30) | copy-start | bytes 3076
  66.0 4.7 %copy-start.9 = (f32[512,4]{0,1:T(4,128)S(1)}, f32[512,4]{0,1:T(4,128)}, u32[]{:S(2)}) copy-start(f32[512,4]{0,1:T(4,128)} %param.24) | copy-start | bytes 24580
  70.8 30.9 %copy-start.1 = (bf16[1024,512]{1,0:T(8,128)(2,1)S(1)}, bf16[1024,512]{1,0:T(8,128)(2,1)}, u32[]{:S(2)}) copy-start(bf16[1024,512]{1,0:T(8,128)(2,1)} %w_ref.1) | copy-start | bytes 3145732
  101.6 1.0 copy-start.2
Sparse Core Ops, SparseCore 0:
  33.2 29.6 all-gather.1
  70.5 31.1 reduce-scatter.1

commit v4 on v3

--- a/solution.py
+++ b/solution.py
@@ -280,6 +280,55 @@
         ),
         cost_estimate=pl.CostEstimate(flops=2**30, bytes_accessed=2**22, transcendentals=0),
     )(head, weight, back)
+
+
+def swap_kernel(count, src_ref, o_ref, rows_in, send_sem, recv_sem):
+    ep = lax.axis_index("ep")
+    mesh_ids = pl.DeviceIdType.MESH
+    barrier = pltpu.get_barrier_semaphore()
+    for d in range(1, count):
+        pl.semaphore_signal(barrier, inc=1, device_id={"ep": lax.rem(ep + d, count)}, device_id_type=mesh_ids)
+    pl.semaphore_wait(barrier, count - 1)
+
+    def row_copy(d):
+        peer = lax.rem(ep + d, count)
+        return pltpu.make_async_remote_copy(
+            src_ref=src_ref.at[peer],
+            dst_ref=rows_in.at[d],
+            send_sem=send_sem.at[d],
+            recv_sem=recv_sem.at[d],
+            device_id={"ep": peer},
+            device_id_type=mesh_ids,
+        )
+
+    for d in range(1, count):
+        row_copy(d).start()
+    o_ref[ep] = src_ref[ep]
+    for d in range(1, count):
+        row_copy(d).wait_recv()
+        o_ref[lax.rem(ep + count - d, count)] = rows_in[d]
+    for d in range(1, count):
+        row_copy(d).wait_send()
+
+
+def swap(blocks):
+    count = lax.axis_size("ep")
+    vm = pl.BlockSpec(memory_space=pltpu.VMEM)
+    return pl.pallas_call(
+        functools.partial(swap_kernel, count),
+        out_shape=jax.ShapeDtypeStruct(blocks.shape, BF),
+        in_specs=[vm],
+        out_specs=vm,
+        scratch_shapes=[
+            pltpu.VMEM(blocks.shape, BF),
+            pltpu.SemaphoreType.DMA((count,)),
+            pltpu.SemaphoreType.DMA((count,)),
+        ],
+        compiler_params=pltpu.CompilerParams(
+            vmem_limit_bytes=16 * 1024 * 1024, collective_id=3, has_side_effects=True
+        ),
+        cost_estimate=pl.CostEstimate(flops=2**27, bytes_accessed=2**22, transcendentals=0),
+    )(blocks)
 
 
 def body(
@@ -343,7 +392,7 @@
         .astype(BF)
         .reshape(expert_count, capacity, share_width)
     )
-    arrived = lax.all_to_all(share_part, "ep", split_axis=0, concat_axis=0, tiled=True)
+    arrived = swap(share_part)
     piece_now = lax.all_gather(arrived, "tp", axis=2, tiled=True)
     piece_now, q_t, k_rows, v_t = lax.optimization_barrier((piece_now, q_t, k_rows, v_t))
     piece_cols = piece_now.shape[2]

time: 144 us -> 142 us (0.986)
  blocking collectives: 18.8 us -> 0 us
  Pallas kernels: 46.3 us -> 59.2 us
  waiting for transfers between devices: 30.4 us -> 34 us
    all_to_all x1 -> x0, blocking collectives: 18.8 us -> none  [body(): lax.all_to_all(share_part, 'ep', split_axis=0, concat_axis=0, tiled=True)]
    pallas_call x0 -> x1, Pallas kernels: none -> 12.9 us  [swap(): pl.pallas_call(functools.partial(swap_kernel, count), out_shape=jax.Shape...]
    all_gather x1, waiting for transfers between devices: 14.7 us -> 18.3 us  [body(): piece_now = lax.all_gather(arrived, 'tp', axis=2, tiled=True)]
where the time goes in v4:
time: 142 us; the launch traced here: 141 us
  Pallas kernels  59.2 us (42%)
  waiting for transfers between devices  34 us (24%)
  between operations  14.4 us (10%)
  matrix products  14.1 us (10%)
  local copies, waits for them, and re-layouts  11.6 us (8%)
  other arithmetic  7.92 us (6%)
    pallas_call x1, Pallas kernels, tail(): pl.pallas_call(functools.partial(tail_kernel, ep_count, tp_count, feats),...  31.1 us
    all_gather x1, waiting for transfers between devices, body(): piece_now = lax.all_gather(arrived, 'tp', axis=2, tiled=True)  18.3 us
    reduce_scatter x1, waiting for transfers between devices, body(): lax.psum_scatter(partial_value, 'tp', scatter_dimension=3, tiled=True)  15.7 us
    pallas_call x1, Pallas kernels, attend(): pl.pallas_call(functools.partial(attend_kernel, heads, count), out_shape=...  15.2 us
    pallas_call x1, Pallas kernels, swap(): pl.pallas_call(functools.partial(swap_kernel, count), out_shape=jax.Shape...  12.9 us
    dot_general x3, matrix products, project(): lax.dot_general(weight, normed, (((0,), (1,)), ((), ())), preferred_eleme...  5.03 us
    mul x3, local copies, waits for them, and re-layouts, head_norm(): x = x * lax.rsqrt(jnp.mean(x * x, axis=1, keepdims=True) + epsilon)  4.97 us
    dot_general x1, matrix products, body(): jnp.einsum('sjcf,jfd->sjcd', hidden, expert_down, preferred_element_type=...  4.28 us
  transfers between devices with their start and end apart: 2, of which 2 were waited for; matrix products, arithmetic and copies ran while one was open for 10% of the time, Pallas kernels for 11%

profile of v4, /device:TPU:0, one launch (start us, length us, event | category | flops | bytes accessed | tf_op | source)
XLA Modules:
  0.0 141.2 jit_solution(11519696444562642992)
XLA Ops:
  7.2 0.9 copy.44
  8.4 2.1 %convert_element_type.57 = f32[128,2048]{1,0:T(8,128)} convert(bf16[128,2048]{1,0:T(8,128)(2,1)} %param.27) | non-fusion elementwise | flops 262144 | bytes 1572864 | tf_op jit(solution)/shard_map/convert_element_type | solution.py:18
  10.8 0.6 reduce-window.6
  12.0 0.9 dynamic-slice
  13.0 1.3 convolution_convert_fusion.1
  14.3 12.9 %shard_map.176 = bf16[8,48,512]{2,1,0:T(8,128)(2,1)} custom-call(bf16[8,48,512]{2,1,0:T(8,128)(2,1)S(1)} %bitcast.83), custom_call_target="tpu_custom_call" | custom-call | flops 134217728 | bytes 4194304 | tf_op jit(solution)/shard_map/pallas_call | solution.py:317
  27.2 2.2 %fusion = f32[512]{0:T(512)S(1)} fusion(bf16[512,2048]{1,0:T(8,128)(2,1)} %param.17), kind=kLoop, calls=%fused_computation.2 | loop fusion | flops 3145216 | bytes 2099200 | tf_op jit(solution)/shard_map/reduce_sum | solution.py:19
  29.4 1.7 %fusion.37 = (f32[256,512]{0,1:T(8,128)}, f32[256,512]{0,1:T(8,128)}) fusion(bf16[2048,256]{1,0:T(8,128)(2,1)S(1)} %copy-done.15, bf16[512,2048]{1,0:T(8,128)(2,1)S(1)} %copy-done.4, f32[2048]{0:T(1024)S(1)} %copy-done.17, f32[512]{0:T(512)S(1)} %add_rsqrt_fusion.2), kind=kOutput, calls=%fused_computation.60 | convolution fusion | flops 541196288 | bytes 4204544 | tf_op jit(solution)/shard_map/dot_general | solution.py:359
  31.2 2.1 %copy.48 = f32[256,512]{1,0:T(8,128)} copy(f32[256,512]{0,1:T(8,128)} %get-tuple-element.22) | data formatting | bytes 1048576 | tf_op jit(solution)/shard_map/mul | solution.py:363
  33.2 1.1 bitcast_reduce_fusion
  34.4 0.9 mul.170
  35.2 2.0 %copy.49 = f32[256,512]{0,1:T(8,128)} copy(f32[256,512]{1,0:T(8,128)} %bitcast.86) | data formatting | bytes 1048576 | tf_op jit(solution)/shard_map/mul | solution.py:363
  37.4 2.4 %bitcast_reduce_fusion.1 = (f32[4,512]{1,0:T(4,128)S(1)}, f32[256,512]{1,0:T(8,128)S(1)}) fusion(bf16[2048,256]{1,0:T(8,128)(2,1)} %param.19, bf16[512,2048]{1,0:T(8,128)(2,1)S(1)} %copy-done.4, f32[2048]{0:T(1024)S(1)} %copy-done.17, f32[512]{0:T(512)S(1)} %add_rsqrt_fusion.2), kind=kOutput, calls=%fused_computation.26 | convolution fusion | flops 541325312 | bytes 3688448 | tf_op jit(solution)/shard_map/dot_general | solution.py:359
  40.1 1.3 copy-done.5
  41.4 0.9 fusion.6.v_ref
  42.3 18.3 %all-gather.2.cloned.1.call-done = bf16[8,48,2048]{2,1,0:T(8,128)(2,1)} async-done(((bf16[8,48,512]{2,1,0:T(8,128)(2,1)}), bf16[8,48,2048]{2,1,0:T(8,128)(2,1)}) %all-gather.2.cloned.1.call-update) | async-done | bytes 1572880 | tf_op jit(solution)/shard_map/all_gather | solution.py:396
  60.7 3.1 %convolution_bitcast_fusion.3 = f32[8,1,48,256]{3,2,0,1:T(8,128)} fusion(bf16[8,48,2048]{2,1,0:T(8,128)(2,1)} %all-gather.2.cloned.1.call-done, bf16[1,2048,256]{2,1,0:T(8,128)(2,1)} %param.31), kind=kOutput, calls=%fused_computation.13 | convolution fusion | flops 402653184 | bytes 3014656 | tf_op jit(solution)/shard_map/sjcd,jdf->sjcf/dot_general | solution.py:400
  63.8 4.3 %fusion.3 = bf16[8,1,48,2048]{3,2,0,1:T(8,128)(2,1)} fusion(bf16[1,256,2048]{2,1,0:T(8,128)(2,1)S(1)} %copy-done, bf16[8,48,2048]{2,1,0:T(8,128)(2,1)S(1)} %copy-done.7, bf16[1,2048,256]{2,1,0:T(8,128)(2,1)} %param.32, f32[8,1,48,256]{3,2,0,1:T(8,128)} %convolution_bitcast_fusion.3), kind=kOutput, calls=%fused_computation.6 | convolution fusion | flops 806682624 | bytes 5636096 | tf_op jit(solution)/shard_map/sjcf,jfd->sjcd/dot_general | solution.py:403
  68.6 15.2 %shard_map.177.head_ref = bf16[512,256]{1,0:T(8,128)(2,1)S(1)} custom-call(bf16[256,512]{1,0:T(8,128)(2,1)S(1)} %fusion.22.q_ref, bf16[512,256]{1,0:T(8,128)(2,1)S(1)} %fusion.21.k_ref, bf16[256,512]{1,0:T(8,128)(2,1)S(1)} %fusion.6.v_ref, f32[8,512]{1,0:T(8,128)S(1)} %pad.4.g_ref, f32[256,1]{1,0:T(8,128)S(1)} %copy.51.gain_ref), custom_call_target="tpu_custom_call" | custom-call | flops 4294967296 | bytes 8388608 | tf_op jit(solution)/shard_map/pallas_call | solution.py:176
  83.8 15.7 %reduce-scatter.2.cloned.1.call-done = bf16[8,1,48,512]{3,2,0,1:T(8,128)(2,1)} async-done(((bf16[8,1,48,2048]{3,2,0,1:T(8,128)(2,1)}), bf16[8,1,48,512]{3,2,0,1:T(8,128)(2,1)}) %reduce-scatter.2.cloned.1.call-update) | async-done | bytes 393232 | tf_op jit(solution)/shard_map/reduce_scatter | solution.py:405
  99.5 1.0 copy-done.2
  100.4 31.1 %shard_map.178 = (bf16[512,512]{1,0:T(8,128)(2,1)S(1)}, bf16[8,48,512]{2,1,0:T(8,128)(2,1)S(1)}) custom-call(bf16[512,256]{1,0:T(8,128)(2,1)S(1)} %shard_map.177.head_ref, bf16[1024,512]{1,0:T(8,128)(2,1)S(1)} %copy-done.1, bf16[8,48,512]{2,1,0:T(8,128)(2,1)S(1)} %bitcast.85), custom_call_target="tpu_custom_call" | custom-call | flops 1073741824 | bytes 4194304 | tf_op jit(solution)/shard_map/pallas_call | solution.py:264
  132.2 1.3 reduce_sum.59
  133.5 0.8 copy.56
  (67 shorter events, 2.7 us)
Async XLA Ops:
  7.2 56.6 %copy-start = (bf16[1,256,2048]{2,1,0:T(8,128)(2,1)S(1)}, bf16[1,256,2048]{2,1,0:T(8,128)(2,1)}, u32[]{:S(2)}) copy-start(bf16[1,256,2048]{2,1,0:T(8,128)(2,1)} %param.33) | copy-start | bytes 3145732
  7.2 4.8 %copy-start.10 = (s32[128,2]{0,1:T(2,128)S(1)}, s32[128,2]{0,1:T(2,128)}, u32[]{:S(2)}) copy-start(s32[128,2]{0,1:T(2,128)} %param.29) | copy-start | bytes 3076
  7.2 3.4 %copy-start.3 = (bf16[128,2048]{1,0:T(8,128)(2,1)S(1)}, bf16[128,2048]{1,0:T(8,128)(2,1)}, u32[]{:S(2)}) copy-start(bf16[128,2048]{1,0:T(8,128)(2,1)} %param.27) | copy-start | bytes 1572868
  7.2 53.5 %all-gather.2.cloned.1.call-start = ((), (), s32[]{:S(2)}) async-start(), calls=%async_computation.1 | async-start | bytes 1966080 | tf_op jit(solution)/shard_map/all_gather | solution.py:396
  11.7 17.7 %copy-start.4 = (bf16[512,2048]{1,0:T(8,128)(2,1)S(1)}, bf16[512,2048]{1,0:T(8,128)(2,1)}, u32[]{:S(2)}) copy-start(bf16[512,2048]{1,0:T(8,128)(2,1)} %param.17) | copy-start | bytes 6291460
  11.7 17.7 %copy-start.17 = (f32[2048]{0:T(1024)S(1)}, f32[2048]{0:T(1024)}, u32[]{:S(2)}) copy-start(f32[2048]{0:T(1024)} %param.18) | copy-start | bytes 24580
  27.2 72.3 %reduce-scatter.2.cloned.1.call-start = ((), (), s32[]{:S(2)}) async-start(), calls=%async_computation.2 | async-start | bytes 1966080 | tf_op jit(solution)/shard_map/reduce_scatter | solution.py:405
  27.2 2.2 %copy-start.15 = (bf16[2048,256]{1,0:T(8,128)(2,1)S(1)}, bf16[2048,256]{1,0:T(8,128)(2,1)}, u32[]{:S(2)}) copy-start(bf16[2048,256]{1,0:T(8,128)(2,1)} %param.20) | copy-start | bytes 3145732
  31.2 6.1 %copy-start.13 = (f32[64]{0:T(128)S(1)}, f32[64]{0:T(128)}, u32[]{:S(2)}) copy-start(f32[64]{0:T(128)} %param.23) | copy-start | bytes 772
  31.2 6.2 %copy-start.14 = (f32[64]{0:T(128)S(1)}, f32[64]{0:T(128)}, u32[]{:S(2)}) copy-start(f32[64]{0:T(128)} %param.22) | copy-start | bytes 772
  37.4 2.5 %copy-start.6 = (f32[256,512]{0,1:T(8,128)S(1)}, f32[256,512]{0,1:T(8,128)}, u32[]{:S(2)}) copy-start(f32[256,512]{0,1:T(8,128)} %copy.49) | copy-start | bytes 1572868
  37.4 2.5 %copy-start.8 = (f32[256,512]{0,1:T(8,128)S(1)}, f32[256,512]{0,1:T(8,128)}, u32[]{:S(2)}) copy-start(f32[256,512]{0,1:T(8,128)} %get-tuple-element.23) | copy-start | bytes 1572868
  37.4 2.6 %copy-start.16 = (bf16[2048,256]{1,0:T(8,128)(2,1)S(1)}, bf16[2048,256]{1,0:T(8,128)(2,1)}, u32[]{:S(2)}) copy-start(bf16[2048,256]{1,0:T(8,128)(2,1)} %param.21) | copy-start | bytes 3145732
  39.8 1.6 %copy-start.5 = (bf16[512,2048]{1,0:T(8,128)(2,1)S(1)}, bf16[512,2048]{1,0:T(8,128)(2,1)}, u32[]{:S(2)}) copy-start(bf16[512,2048]{1,0:T(8,128)(2,1)} %param.17) | copy-start | bytes 6291460
  60.7 3.1 %copy-start.7 = (bf16[8,48,2048]{2,1,0:T(8,128)(2,1)S(1)}, bf16[8,48,2048]{2,1,0:T(8,128)(2,1)}, u32[]{:S(2)}) copy-start(bf16[8,48,2048]{2,1,0:T(8,128)(2,1)} %all-gather.2.cloned.1.call-done) | copy-start | bytes 4718596
  63.8 4.3 %copy-start.11 = (f32[256]{0:T(256)S(1)}, f32[256]{0:T(256)}, u32[]{:S(2)}) copy-start(f32[256]{0:T(256)} %param.25) | copy-start | bytes 3076
  63.8 4.5 %copy-start.12 = (f32[128,2]{0,1:T(2,128)S(1)}, f32[128,2]{0,1:T(2,128)}, u32[]{:S(2)}) copy-start(f32[128,2]{0,1:T(2,128)} %param.30) | copy-start | bytes 3076
  63.8 4.7 %copy-start.9 = (f32[512,4]{0,1:T(4,128)S(1)}, f32[512,4]{0,1:T(4,128)}, u32[]{:S(2)}) copy-start(f32[512,4]{0,1:T(4,128)} %param.24) | copy-start | bytes 24580
  68.6 30.9 %copy-start.1 = (bf16[1024,512]{1,0:T(8,128)(2,1)S(1)}, bf16[1024,512]{1,0:T(8,128)(2,1)}, u32[]{:S(2)}) copy-start(bf16[1024,512]{1,0:T(8,128)(2,1)} %w_ref.1) | copy-start | bytes 3145732
  99.5 1.0 copy-start.2
Sparse Core Ops, SparseCore 0:
  27.3 33.3 all-gather.1
  68.3 31.1 reduce-scatter.1
